TPU v7x, 256 devices: a whole 4x4x8 slice. The times are simulated.
256 devices in a mesh: ep: 16 (over y, x), tp: 16 (over z, core).
Axes of the slice: x: 4, y: 4, z: 8, core: 2. Of those that a mesh axis runs over, the one named last changes fastest.
Arguments:
- mix_query: bfloat16 [16384, 2048], P('ep', 'tp'), may hold values from -60 to 60
- mix_key: bfloat16 [16384, 2048], P('ep', 'tp'), may hold values from -60 to 60
- mix_value: bfloat16 [16384, 2048], P('ep', 'tp'), may hold values from -6 to 6
- head_lambda: float32 [16], P('tp'), may hold values from 0.3 to 0.8
- head_gain: float32 [128], replicated, may hold values from 0.1 to 1.9
- out_weight: bfloat16 [2048, 2048], P('tp'), may hold values from -0.125 to 0.125
- moe_input: bfloat16 [16384, 2048], P(('ep', 'tp')), may hold values from -6 to 6
- moe_gain: float32 [2048], replicated, may hold values from 0.1 to 1.9
- expert_ids: int32 [16384, 2], P(('ep', 'tp')), may hold values from 0 to 15, all different within a row; in each aligned block of 64 rows (0 to 63, 64 to 127, ...) at most 12 rows name the same one
- route_weight: float32 [16384, 2], P(('ep', 'tp')), may hold values from 0.2 to 1
- gate_weight: bfloat16 [16, 2048, 4096], P('ep', None, 'tp'), may hold values from -0.125 to 0.125
- up_weight: bfloat16 [16, 2048, 4096], P('ep', None, 'tp'), may hold values from -0.125 to 0.125
- down_weight: bfloat16 [16, 4096, 2048], P('ep', 'tp'), may hold values from -0.09375 to 0.09375
Outputs:
- mix_output: bfloat16 [16384, 2048], P(('ep', 'tp'))
- moe_output: bfloat16 [16384, 2048], P(('ep', 'tp'))
Inputs may be any that keep to these rules, and one draw needn't show every extreme that they name: `expert_ids`: in each aligned block of 64 rows (the rows of one device) no expert is named by more than 12 rows; a row names 2 different experts.
All inputs are finite; a program needn't handle non-finite values.
Results may differ from a plain program's by a relative error of at most 0.02.
The roundings to bfloat16 on the way count: a program that leaves them out, or rounds other values in their place, can miss the bound.
Values may be sent and summed in bfloat16 or wider, within the bound.
A program may use at most 128 MiB of HBM per device.

v0:
```python
import math

import jax
import jax.numpy as jnp
from jax import lax
from jax.sharding import PartitionSpec as P

epsilon = 1e-06
rotary_base = 10000.0
far_below = -1e30


def norm_rows(values, scales):
    square_mean = jnp.mean(values * values, axis=-1, keepdims=True)
    return values * lax.rsqrt(square_mean + epsilon) * scales


def rotate(values, positions):
    half_dim = values.shape[-1] // 2
    frequency = rotary_base ** (-jnp.arange(half_dim, dtype=jnp.float32) * 2.0 / values.shape[-1])
    angles = positions.astype(jnp.float32)[:, None] * frequency[None, :]
    layout = (values.shape[0],) + (1,) * (values.ndim - 2) + (half_dim,)
    cosine = jnp.cos(angles).reshape(layout)
    sine_table = jnp.sin(angles).reshape(layout)
    leading = values[..., :half_dim]
    trailing = values[..., half_dim:]
    return jnp.concatenate(
        [leading * cosine - trailing * sine_table, trailing * cosine + leading * sine_table],
        axis=-1,
    )


def attend_block(attention_state, key_rows, value_rows, key_pos, queries, query_pos):
    running_max, totals, weighted = attention_state
    scores = jnp.einsum("qhpd,khpd->hpqk", queries, key_rows, preferred_element_type=jnp.float32)
    visible = (key_pos[None, :] <= query_pos[:, None])[None, None, :, :]
    new_max = jnp.maximum(running_max, jnp.max(jnp.where(visible, scores, far_below), axis=-1))
    expo = jnp.where(visible, jnp.exp(scores - new_max[..., None]), 0.0)
    shrink = jnp.exp(running_max - new_max)
    totals = totals * shrink + jnp.sum(expo, axis=-1)
    weighted = weighted * shrink[..., None] + jnp.einsum(
        "hpqk,khe->hpqe", expo.astype(jnp.bfloat16), value_rows, preferred_element_type=jnp.float32
    )
    return (new_max, totals, weighted)


def fold_keys(attention_state, stacked, queries, query_pos, query_last):
    heads_here = queries.shape[1]
    head_size = queries.shape[3]
    number = stacked.shape[0]
    step_rows = math.gcd(number, 1024)
    key_cols = heads_here * 2 * head_size

    def one_block(block_index, running):
        row_begin = block_index * step_rows
        key_block = lax.dynamic_slice_in_dim(stacked, row_begin, step_rows, 0)
        key_rows = key_block[:, :key_cols].reshape(step_rows, heads_here, 2, head_size)
        value_rows = key_block[:, key_cols:].reshape(step_rows, heads_here, -1)
        key_pos = row_begin + jnp.arange(step_rows, dtype=jnp.int32)

        def update(unchanged):
            return attend_block(unchanged, key_rows, value_rows, key_pos, queries, query_pos)

        def keep(unchanged):
            return unchanged

        return lax.cond(jnp.min(key_pos) > query_last, keep, update, running)

    return lax.fori_loop(0, number // step_rows, one_block, attention_state)


def body(
    mix_query,
    mix_key,
    mix_value,
    head_lambda,
    head_gain,
    out_weight,
    moe_input,
    moe_gain,
    expert_ids,
    route_weight,
    gate_weight,
    up_weight,
    down_weight,
):
    seq_rows = mix_query.shape[0]
    heads_here = head_lambda.shape[0]
    head_size = mix_query.shape[1] // (2 * heads_here)
    value_size = mix_value.shape[1] // heads_here
    ep_size = lax.axis_size("ep")
    tp_size = lax.axis_size("tp")
    my_shard = lax.axis_index("ep")
    query_pos = my_shard * seq_rows + jnp.arange(seq_rows, dtype=jnp.int32)
    queries = rotate(
        mix_query.astype(jnp.float32).reshape(seq_rows, heads_here, 2, head_size), query_pos
    )
    queries = (queries * head_size ** (-0.5)).astype(jnp.bfloat16)
    rotated_keys = rotate(
        mix_key.astype(jnp.float32).reshape(seq_rows, heads_here, 2, head_size), query_pos
    )
    rotated_keys = rotated_keys.astype(jnp.bfloat16).reshape(seq_rows, heads_here * 2 * head_size)
    stacked = jnp.concatenate([rotated_keys, mix_value], axis=1)
    query_last = jnp.max(query_pos)
    initial = (
        jnp.full((heads_here, 2, seq_rows), far_below, jnp.float32),
        jnp.zeros((heads_here, 2, seq_rows), jnp.float32),
        jnp.zeros((heads_here, 2, seq_rows, value_size), jnp.float32),
    )
    attention_state = fold_keys(
        initial, lax.all_gather(stacked, "ep", axis=0, tiled=True), queries, query_pos, query_last
    )
    running_max, totals, weighted = attention_state
    lambdas = head_lambda[:, None, None]
    combined_heads = (
        weighted[:, 0] / totals[:, 0][..., None]
        - lambdas * weighted[:, 1] / totals[:, 1][..., None]
    )
    combined_heads = norm_rows(combined_heads, head_gain).astype(jnp.bfloat16)
    head_rows = jnp.transpose(combined_heads, (1, 0, 2)).reshape(seq_rows, heads_here * value_size)
    rows_b = moe_input.shape[0]
    top_count = expert_ids.shape[1]
    exp_here = gate_weight.shape[0]
    experts = exp_here * ep_size
    slot_count = 3 * rows_b * top_count // (2 * experts)
    normed = norm_rows(moe_input.astype(jnp.float32), moe_gain).astype(jnp.bfloat16)
    flat_ids = expert_ids.reshape(rows_b * top_count)
    member = (flat_ids[:, None] == jnp.arange(experts, dtype=jnp.int32)[None, :]).astype(jnp.int32)
    slot_rank = jnp.sum(member * (jnp.cumsum(member, axis=0) - 1), axis=1)
    target = (slot_rank * experts + flat_ids).reshape(rows_b, top_count)
    selector = (
        jnp.transpose(target)[:, :, None]
        == jnp.arange(slot_count * experts, dtype=jnp.int32)[None, None, :]
    ).astype(jnp.bfloat16)
    dispatched = jnp.einsum(
        "krs,rd->sd", selector, normed, preferred_element_type=jnp.float32
    ).astype(jnp.bfloat16)
    outgoing = dispatched.reshape(1, slot_count, experts, -1)
    arrived = lax.all_to_all(outgoing, "ep", split_axis=2, concat_axis=0, tiled=True)
    expert_rows = arrived.reshape(ep_size * slot_count, exp_here, -1)
    row_block = lax.all_gather(expert_rows, "tp", axis=0, tiled=True)
    gate_act = jnp.einsum(
        "mxd,xdf->mxf", row_block, gate_weight, preferred_element_type=jnp.float32
    )
    upper = jnp.einsum("mxd,xdf->mxf", row_block, up_weight, preferred_element_type=jnp.float32)
    hidden = (jax.nn.silu(gate_act) * upper).astype(jnp.bfloat16)
    rows_a = seq_rows // tp_size
    rows_e = ep_size * slot_count
    per_device = rows_a + rows_e * exp_here
    blocks = lax.axis_size("tp") * per_device // per_device
    mixer_part = jnp.dot(head_rows, out_weight, preferred_element_type=jnp.float32).reshape(
        blocks, rows_a, -1
    )
    row_block = hidden
    expert_part = jnp.einsum(
        "mxf,xfd->mxd", row_block, down_weight, preferred_element_type=jnp.float32
    ).reshape(blocks, rows_e * exp_here, -1)
    joined = lax.psum_scatter(
        jnp.concatenate([mixer_part, expert_part], axis=1)
        .reshape(lax.axis_size("tp") * per_device, -1)
        .astype(jnp.bfloat16),
        "tp",
        scatter_dimension=0,
        tiled=True,
    ).astype(jnp.float32)
    mix_sum = joined[:rows_a]
    expert_sum = joined[rows_a:].reshape(rows_e, exp_here, -1)
    mix_rows = mix_sum.astype(jnp.bfloat16)
    returning = expert_sum.astype(jnp.bfloat16).reshape(ep_size, slot_count, exp_here, -1)
    returned = lax.all_to_all(returning, "ep", split_axis=0, concat_axis=2, tiled=True)
    results = returned.reshape(slot_count * experts, -1)
    chosen = jnp.einsum("krs,sd->krd", selector, results, preferred_element_type=jnp.float32)
    combined = jnp.sum(chosen * jnp.transpose(route_weight)[:, :, None], axis=0)
    return (mix_rows, combined.astype(jnp.bfloat16))


def solution(mesh):
    return jax.shard_map(
        body,
        mesh=mesh,
        in_specs=(
            P("ep", "tp"),
            P("ep", "tp"),
            P("ep", "tp"),
            P("tp"),
            P(),
            P("tp", None),
            P(("ep", "tp"), None),
            P(),
            P(("ep", "tp"), None),
            P(("ep", "tp"), None),
            P("ep", None, "tp"),
            P("ep", None, "tp"),
            P("ep", "tp", None),
        ),
        out_specs=(P(("ep", "tp"), None), P(("ep", "tp"), None)),
        check_vma=False,
    )
```

profile of v0, /device:TPU:16, one launch (start us, length us, event | category | flops | bytes accessed | tf_op | source)
XLA Modules:
  0.0 446.2 jit_solution(10264336150292983697)
XLA Ops:
  17.0 29.0 %all_to_all.30 = bf16[1,12,16,2048]{3,1,0,2:T(8,128)(2,1)S(1)} all-to-all(bf16[1,12,16,2048]{3,1,0,2:T(8,128)(2,1)S(1)} %copy.42), channel_id=1, replica_groups=mesh['ep'=16,'tp'=16] {'ep'}, dimensions={2} | all-to-all | bytes 1572864 | tf_op jit(solution)/shard_map/all_to_all | solution.py:139
  48.7 48.6 %all-gather.3.cloned.1.call-done = bf16[16384,256]{1,0:T(8,128)(2,1)} async-done(((bf16[1024,256]{1,0:T(8,128)(2,1)}), bf16[16384,256]{1,0:T(8,128)(2,1)}) %all-gather.3.cloned.1.call-update) | async-done | bytes 8388624 | tf_op jit(solution)/shard_map/all_gather | solution.py:111
  97.4 109.8 %while.18 = (s32[]{:T(128)}, f32[1,2,1024]{2,1,0:T(2,128)S(1)}, f32[1,2,1024]{2,1,0:T(2,128)S(1)}, f32[1,2,1024,128]{3,2,1,0:T(8,128)S(1)}, s32[]{:T(128)}, /*in...) while((s32[]{:T(128)}, f32[1,2,1024]{2,1,0:T(2,128)S(1)}, ...), condition=%wide.region_7.8_spmd.clone, body=%wide.region_1.7_spmd.clone.sunk | while | flops 823665664 | bytes 33448252 | solution.py:69
  99.3 8.6 %conditional.3 = (f32[1,2,1024]{2,1,0:T(2,128)S(1)}, f32[1,2,1024]{2,1,0:T(2,128)S(1)}, f32[1,2,1024,128]{3,2,1,0:T(8,128)S(1)}) conditional(s32[]{:T(128)} %convert_element_type.127, (s32[1024]{0:T(1024)S(1)}, s32[]{:T(128)}, s32[]{:T(128)}, bf16[16384,256]{1,0:T(8,128)(2,1)}, bf16[1024,1,2,64]{0,3,2,1:T(8,128)(2,1)S(1)}, ...), branch_computations={%region_3.5_spmd, %region_6.6_spmd} | conditional | flops 823663616 | bytes 33423446 | solution.py:67
  102.8 3.4 fusion.15
  110.0 8.7 %conditional.3 = (f32[1,2,1024]{2,1,0:T(2,128)S(1)}, f32[1,2,1024]{2,1,0:T(2,128)S(1)}, f32[1,2,1024,128]{3,2,1,0:T(8,128)S(1)}) conditional(s32[]{:T(128)} %convert_element_type.127, (s32[1024]{0:T(1024)S(1)}, s32[]{:T(128)}, s32[]{:T(128)}, bf16[16384,256]{1,0:T(8,128)(2,1)}, bf16[1024,1,2,64]{0,3,2,1:T(8,128)(2,1)S(1)}, ...), branch_computations={%region_3.5_spmd, %region_6.6_spmd} | conditional | flops 823663616 | bytes 33423446 | solution.py:67
  113.5 3.4 fusion.15
  120.6 8.6 %conditional.3 = (f32[1,2,1024]{2,1,0:T(2,128)S(1)}, f32[1,2,1024]{2,1,0:T(2,128)S(1)}, f32[1,2,1024,128]{3,2,1,0:T(8,128)S(1)}) conditional(s32[]{:T(128)} %convert_element_type.127, (s32[1024]{0:T(1024)S(1)}, s32[]{:T(128)}, s32[]{:T(128)}, bf16[16384,256]{1,0:T(8,128)(2,1)}, bf16[1024,1,2,64]{0,3,2,1:T(8,128)(2,1)S(1)}, ...), branch_computations={%region_3.5_spmd, %region_6.6_spmd} | conditional | flops 823663616 | bytes 33423446 | solution.py:67
  124.1 3.4 fusion.15
  131.2 8.6 %conditional.3 = (f32[1,2,1024]{2,1,0:T(2,128)S(1)}, f32[1,2,1024]{2,1,0:T(2,128)S(1)}, f32[1,2,1024,128]{3,2,1,0:T(8,128)S(1)}) conditional(s32[]{:T(128)} %convert_element_type.127, (s32[1024]{0:T(1024)S(1)}, s32[]{:T(128)}, s32[]{:T(128)}, bf16[16384,256]{1,0:T(8,128)(2,1)}, bf16[1024,1,2,64]{0,3,2,1:T(8,128)(2,1)S(1)}, ...), branch_computations={%region_3.5_spmd, %region_6.6_spmd} | conditional | flops 823663616 | bytes 33423446 | solution.py:67
  134.7 3.4 fusion.15
  141.8 8.7 %conditional.3 = (f32[1,2,1024]{2,1,0:T(2,128)S(1)}, f32[1,2,1024]{2,1,0:T(2,128)S(1)}, f32[1,2,1024,128]{3,2,1,0:T(8,128)S(1)}) conditional(s32[]{:T(128)} %convert_element_type.127, (s32[1024]{0:T(1024)S(1)}, s32[]{:T(128)}, s32[]{:T(128)}, bf16[16384,256]{1,0:T(8,128)(2,1)}, bf16[1024,1,2,64]{0,3,2,1:T(8,128)(2,1)S(1)}, ...), branch_computations={%region_3.5_spmd, %region_6.6_spmd} | conditional | flops 823663616 | bytes 33423446 | solution.py:67
  152.5 8.7 %conditional.3 = (f32[1,2,1024]{2,1,0:T(2,128)S(1)}, f32[1,2,1024]{2,1,0:T(2,128)S(1)}, f32[1,2,1024,128]{3,2,1,0:T(8,128)S(1)}) conditional(s32[]{:T(128)} %convert_element_type.127, (s32[1024]{0:T(1024)S(1)}, s32[]{:T(128)}, s32[]{:T(128)}, bf16[16384,256]{1,0:T(8,128)(2,1)}, bf16[1024,1,2,64]{0,3,2,1:T(8,128)(2,1)S(1)}, ...), branch_computations={%region_3.5_spmd, %region_6.6_spmd} | conditional | flops 823663616 | bytes 33423446 | solution.py:67
  156.0 3.4 fusion.15
  163.2 8.6 %conditional.3 = (f32[1,2,1024]{2,1,0:T(2,128)S(1)}, f32[1,2,1024]{2,1,0:T(2,128)S(1)}, f32[1,2,1024,128]{3,2,1,0:T(8,128)S(1)}) conditional(s32[]{:T(128)} %convert_element_type.127, (s32[1024]{0:T(1024)S(1)}, s32[]{:T(128)}, s32[]{:T(128)}, bf16[16384,256]{1,0:T(8,128)(2,1)}, bf16[1024,1,2,64]{0,3,2,1:T(8,128)(2,1)S(1)}, ...), branch_computations={%region_3.5_spmd, %region_6.6_spmd} | conditional | flops 823663616 | bytes 33423446 | solution.py:67
  173.8 8.6 %conditional.3 = (f32[1,2,1024]{2,1,0:T(2,128)S(1)}, f32[1,2,1024]{2,1,0:T(2,128)S(1)}, f32[1,2,1024,128]{3,2,1,0:T(8,128)S(1)}) conditional(s32[]{:T(128)} %convert_element_type.127, (s32[1024]{0:T(1024)S(1)}, s32[]{:T(128)}, s32[]{:T(128)}, bf16[16384,256]{1,0:T(8,128)(2,1)}, bf16[1024,1,2,64]{0,3,2,1:T(8,128)(2,1)S(1)}, ...), branch_computations={%region_3.5_spmd, %region_6.6_spmd} | conditional | flops 823663616 | bytes 33423446 | solution.py:67
  184.4 8.6 %conditional.3 = (f32[1,2,1024]{2,1,0:T(2,128)S(1)}, f32[1,2,1024]{2,1,0:T(2,128)S(1)}, f32[1,2,1024,128]{3,2,1,0:T(8,128)S(1)}) conditional(s32[]{:T(128)} %convert_element_type.127, (s32[1024]{0:T(1024)S(1)}, s32[]{:T(128)}, s32[]{:T(128)}, bf16[16384,256]{1,0:T(8,128)(2,1)}, bf16[1024,1,2,64]{0,3,2,1:T(8,128)(2,1)S(1)}, ...), branch_computations={%region_3.5_spmd, %region_6.6_spmd} | conditional | flops 823663616 | bytes 33423446 | solution.py:67
  208.0 4.0 convolution_convert_fusion.1
  212.0 10.0 %fusion.27 = f32[3072,1,256]{2,0,1:T(8,128)} fusion(bf16[3072,1,2048]{2,0,1:T(8,128)(2,1)} %all-gather.5.cloned.1.call-done, bf16[1,2048,256]{2,1,0:T(8,128)(2,1)} %param.27), kind=kOutput, calls=%fused_computation.33 | convolution fusion | flops 3221225472 | bytes 16777216 | tf_op jit(solution)/shard_map/mxd,xdf->mxf/dot_general | solution.py:142
  222.0 19.0 %convolution_convert_fusion = bf16[3072,2048]{1,0:T(8,128)(2,1)} fusion(bf16[3072,1,2048]{2,0,1:T(8,128)(2,1)} %all-gather.5.cloned.1.call-done, f32[3072,1,256]{2,0,1:T(8,128)} %fusion.27, bf16[1,256,2048]{2,1,0:T(8,128)(2,1)S(1)} %copy-done, bf16[1,2048,256]{2,1,0:T(8,128)(2,1)S(1)} %copy-done.2), kind=kOutput, calls=%fused_computation.32 | convolution fusion | flops 6453460992 | bytes 30408704 | tf_op jit(solution)/shard_map/mxf,xfd->mxd/dot_general | solution.py:155
  241.0 13.8 %pad_maximum_fusion = bf16[16,256,2048]{2,1,0:T(8,128)(2,1)} fusion(bf16[16,192,2048]{2,1,0:T(8,128)(2,1)} %bitcast.145, bf16[16,64,2048]{2,1,0:T(8,128)(2,1)} %convolution_convert_fusion.1), kind=kLoop, calls=%fused_computation.27 | loop fusion | flops 33554432 | bytes 33554432 | tf_op jit(solution)/shard_map/concatenate | solution.py:159
  254.9 159.8 %reduce-scatter.2.cloned.1.call-done = bf16[256,2048]{1,0:T(8,128)(2,1)} async-done(((bf16[4096,2048]{1,0:T(8,128)(2,1)}), bf16[256,2048]{1,0:T(8,128)(2,1)}) %reduce-scatter.2.cloned.1.call-update) | async-done | bytes 1048592 | tf_op jit(solution)/shard_map/reduce_scatter | solution.py:158
  417.1 7.2 %all-to-all-start.1 = ((bf16[16,12,1,2048]{3,1,2,0:T(8,128)(2,1)}), bf16[16,12,1,2048]{3,1,2,0:T(8,128)(2,1)S(1)}, u32[]{:S(2)}, u32[]{:S(2)}) async-start(bf16[16,12,1,2048]{3,1,2,0:T(8,128)(2,1)} %bitcast.42), calls=%async_computation.2 | async-start | bytes 2097152 | tf_op jit(solution)/shard_map/all_to_all | solution.py:170
  426.0 12.2 %all-to-all-done.1 = bf16[16,12,1,2048]{3,1,2,0:T(8,128)(2,1)S(1)} async-done(((bf16[16,12,1,2048]{3,1,2,0:T(8,128)(2,1)}), bf16[16,12,1,2048]{3,1,2,0:T(8,128)(2,1)S(1)}, u32[]{:S(2)}, u32[]{:S(2)}) %all-to-all-start.1) | async-done | bytes 786464 | tf_op jit(solution)/shard_map/all_to_all | solution.py:170
  (194 shorter events, 88.9 us)
Async XLA Ops:
  7.2 214.9 %copy-start = (bf16[1,256,2048]{2,1,0:T(8,128)(2,1)S(1)}, bf16[1,256,2048]{2,1,0:T(8,128)(2,1)}, u32[]{:S(2)}) copy-start(bf16[1,256,2048]{2,1,0:T(8,128)(2,1)} %param.29) | copy-start | bytes 3145732
  7.2 90.1 %all-gather.3.cloned.1.call-start = ((), (), s32[]{:S(2)}) async-start(), calls=%async_computation.3 | async-start | bytes 8912896 | tf_op jit(solution)/shard_map/all_gather | solution.py:111
  12.2 199.8 %all-gather.5.cloned.1.call-start = ((), (), s32[]{:S(2)}) async-start(), calls=%async_computation.4 | async-start | bytes 13369344 | tf_op jit(solution)/shard_map/all_gather | solution.py:141
  47.1 367.6 %reduce-scatter.2.cloned.1.call-start = ((), (), s32[]{:S(2)}) async-start(), calls=%async_computation.5 | async-start | bytes 17825792 | tf_op jit(solution)/shard_map/reduce_scatter | solution.py:158
  97.4 110.6 %copy-start.1 = (f32[128]{0:T(128)S(1)}, f32[128]{0:T(128)}, u32[]{:S(2)}) copy-start(f32[128]{0:T(128)} %param.21) | copy-start | bytes 1540
  212.0 10.0 %copy-start.2 = (bf16[1,2048,256]{2,1,0:T(8,128)(2,1)S(1)}, bf16[1,2048,256]{2,1,0:T(8,128)(2,1)}, u32[]{:S(2)}) copy-start(bf16[1,2048,256]{2,1,0:T(8,128)(2,1)} %param.28) | copy-start | bytes 3145732
  254.9 183.7 %copy-start.3 = (f32[64,2]{0,1:T(2,128)S(1)}, f32[64,2]{0,1:T(2,128)}, u32[]{:S(2)}) copy-start(f32[64,2]{0,1:T(2,128)} %param.26) | copy-start | bytes 1540
  417.1 21.1 %all-to-all-start.1 = ((bf16[16,12,1,2048]{3,1,2,0:T(8,128)(2,1)}), bf16[16,12,1,2048]{3,1,2,0:T(8,128)(2,1)S(1)}, u32[]{:S(2)}, u32[]{:S(2)}) async-start(bf16[16,12,1,2048]{3,1,2,0:T(8,128)(2,1)} %bitcast.42), calls=%async_computation.2 | async-start | bytes 2097152 | tf_op jit(solution)/shard_map/all_to_all | solution.py:170
Sparse Core Ops, SparseCore 0:
  12.4 84.8 all-gather.2
  99.1 75.3 all-gather.4
  255.0 159.6 reduce-scatter.1
where the time goes:
time: 452 us; the launch traced here: 446 us
  waiting for transfers between devices  221 us (49%)
  matrix products  80.7 us (18%)
  other arithmetic  51.2 us (11%)
  blocking collectives  29 us (6%)
  loops' own time  22.3 us (5%)
  local copies, waits for them, and re-layouts  20.2 us (4%)
  between operations  14.6 us (3%)
  starting transfers between devices  7.52 us (2%)
    reduce_scatter x1, waiting for transfers between devices, body(): lax.psum_scatter(jnp.concatenate([mixer_part, expert_part], axis=1).resha...  160 us
    all_gather x1, waiting for transfers between devices, body(): lax.all_gather(stacked, 'ep', axis=0, tiled=True)  48.6 us
    dot_general x9, matrix products, attend_block(): jnp.einsum('hpqk,khe->hpqe', expo.astype(jnp.bfloat16), value_rows, prefe...  30.4 us
    all_to_all x1, blocking collectives, body(): lax.all_to_all(outgoing, 'ep', split_axis=2, concat_axis=0, tiled=True)  29 us
    another operation x1, loops' own time, fold_keys(): return lax.fori_loop(0, number // step_rows, one_block, attention_state)  21.4 us
    dot_general x1, matrix products, body(): jnp.einsum('mxf,xfd->mxd', row_block, down_weight, preferred_element_type...  19 us
    reduce_sum x9, other arithmetic, attend_block(): totals = totals * shrink + jnp.sum(expo, axis=-1)  15.4 us
    dot_general x9, matrix products, attend_block(): jnp.einsum('qhpd,khpd->hpqk', queries, key_rows, preferred_element_type=j...  14.9 us
  transfers between devices with their start and end apart: 4, of which 3 were waited for; matrix products, arithmetic and copies ran while one was open for 23% of the time, Pallas kernels for 0%

commit v1 on v0

v1 whole, which is shorter than its diff:
```python
import functools

import jax
import jax.numpy as jnp
from jax import lax
from jax.experimental import pallas as pl
from jax.experimental.pallas import tpu as pltpu
from jax.sharding import PartitionSpec as P

epsilon = 1e-06
rotary_base = 10000.0
far_below = -1e30
MESH = pl.DeviceIdType.MESH
F32 = jnp.float32
BF16 = jnp.bfloat16
PAD = 16


def remote(src, dst, send, recv, ep, tp):
    return pltpu.make_async_remote_copy(
        src_ref=src, dst_ref=dst, send_sem=send, recv_sem=recv,
        device_id={"ep": ep, "tp": tp}, device_id_type=MESH,
    )


def kernel(cfg, *refs):
    (NE, NZ, SL, DM, FFD, ROWS, CAP) = cfg
    (q_hbm, k_hbm, v_hbm, lam_ref, gain_ref, wo_hbm, x_hbm, mgain_ref, ids_ref, rw_ref,
     wg_hbm, wu_hbm, wd_hbm, cos_ref, sin_ref,
     mix_ref, moe_ref,
     xin, q_in, k_in, v_in, wg, wu, wd, wo, disp, A, X, Y, RU, RD, RET, B,
     KA, VT, Q2, acc, m_s, l_s, hb, hx, MY, MRU, MRD,
     in_sem, wsend, wrecv, dsend, drecv, kvsend, kvrecv,
     agus, agur, agds, agdr, rsus, rsur, rsds, rsdr, rtsend, rtrecv, hsend, hrecv,
     mus, mur, mds, mdr) = refs

    E = lax.axis_index("ep")
    T = lax.axis_index("tp")
    Z = T // 2
    C = T % 2
    up_t = 2 * ((Z + 1) % NZ) + C
    dn_t = 2 * ((Z + NZ - 1) % NZ) + C
    par_t = 2 * Z + (1 - C)
    SLOTS = NE * CAP
    HALF = SLOTS // 2
    HEADS_W = 128
    PS = NE * PAD

    def local(src, dst, i):
        return pltpu.make_async_copy(src, dst, in_sem.at[i])

    c_x = local(x_hbm, xin, 0)
    c_k = local(k_hbm, k_in, 1)
    c_v = local(v_hbm, v_in, 2)
    c_q = local(q_hbm, q_in, 3)
    c_w = [local(wg_hbm.at[0], wg.at[0], 4), local(wu_hbm.at[0], wu.at[0], 5),
           local(wd_hbm.at[0], wd.at[0], 6), local(wo_hbm, wo.at[0], 7)]
    for c in (c_x, c_k, c_v, c_q, *c_w):
        c.start()

    barrier = pltpu.get_barrier_semaphore()

    def greet(j, _):
        pl.semaphore_signal(barrier, inc=1, device_id={"ep": (E + j) % NE, "tp": T}, device_id_type=MESH)
        return 0

    lax.fori_loop(1, NE, greet, 0)
    for t in (up_t, dn_t, par_t):
        pl.semaphore_signal(barrier, inc=1, device_id={"ep": E, "tp": t}, device_id_type=MESH)

    ids = ids_ref[...]
    lane = lax.broadcasted_iota(jnp.int32, (ROWS, 128), 1)
    hot = [(ids[:, j:j + 1] == lane).astype(F32) for j in range(2)]
    r_i = lax.broadcasted_iota(jnp.int32, (ROWS, ROWS), 0)
    c_i = lax.broadcasted_iota(jnp.int32, (ROWS, ROWS), 1)
    below = (c_i < r_i).astype(BF16)
    before = jnp.dot(below, (hot[0] + hot[1]).astype(BF16), preferred_element_type=F32)
    slot_lane = lax.broadcasted_iota(jnp.int32, (ROWS, PS), 1)
    sel = []
    for j in range(2):
        rank = jnp.sum(hot[j] * before, axis=1, keepdims=True).astype(jnp.int32)
        slot = ids[:, j:j + 1] * PAD + rank
        sel.append((slot == slot_lane).astype(BF16))

    c_x.wait()
    xv = xin[...].astype(F32)
    normed = (xv * lax.rsqrt(jnp.mean(xv * xv, axis=-1, keepdims=True) + epsilon) * mgain_ref[...]).astype(BF16)
    both = sel[0] + sel[1]
    for n in range(0, DM, 512):
        nn = min(512, DM)
        disp[:, n:n + nn] = lax.dot_general(
            both, normed[:, n:n + nn], (((0,), (0,)), ((), ())), preferred_element_type=F32
        ).astype(BF16)

    pl.semaphore_wait(barrier, NE - 1 + 3)

    def rows_of(buf, e):
        return buf.at[pl.ds(pl.multiple_of(e * PAD, PAD), PAD)]

    def disp_copy(j):
        dst = (E + j) % NE
        return remote(rows_of(disp, dst), rows_of(A, E), dsend.at[j], drecv.at[E], dst, T)

    def send_disp(j, _):
        disp_copy(j).start()
        return 0

    lax.fori_loop(1, NE, send_disp, 0)
    own = pl.ds(pl.multiple_of(E * PAD, PAD), PAD)
    A[own, :] = disp[own, :]

    w_copies = [
        remote(wg_hbm.at[0], wg.at[1], wsend.at[0], wrecv.at[0], E, par_t),
        remote(wu_hbm.at[0], wu.at[1], wsend.at[1], wrecv.at[1], E, par_t),
        remote(wd_hbm.at[0], wd.at[1], wsend.at[2], wrecv.at[2], E, par_t),
        remote(wo_hbm, wo.at[1], wsend.at[3], wrecv.at[3], E, par_t),
    ]
    for c in w_copies:
        c.start()

    cosv, sinv = cos_ref[...], sin_ref[...]

    def rotated(xt):
        parts = []
        for m in range(2):
            a = xt[64 * m:64 * m + 32, :]
            b = xt[64 * m + 32:64 * m + 64, :]
            parts.append(a * cosv - b * sinv)
            parts.append(b * cosv + a * sinv)
        return jnp.concatenate(parts, axis=0)

    c_k.wait()
    kt = rotated(k_in[...].astype(F32).T)
    KA[E] = kt.T.astype(BF16)
    c_v.wait()
    VT[E] = v_in[...].T

    def kv_copies(j):
        dst = (E + j) % NE
        return (remote(KA.at[E], KA.at[E], kvsend.at[0, j], kvrecv.at[0, E], dst, T),
                remote(VT.at[E], VT.at[E], kvsend.at[1, j], kvrecv.at[1, E], dst, T))

    def send_kv(j, _):
        @pl.when(E + j < NE)
        def _():
            for c in kv_copies(j):
                c.start()
        return 0

    lax.fori_loop(1, NE, send_kv, 0)

    c_q.wait()
    qt = (rotated(q_in[...].astype(F32).T) * 64 ** (-0.5)).astype(BF16)
    zero = jnp.zeros((64, SL), BF16)
    Q2[:, :SL] = jnp.concatenate([qt[:64], zero], axis=0)
    Q2[:, SL:] = jnp.concatenate([zero, qt[64:]], axis=0)
    acc[...] = jnp.zeros(acc.shape, F32)
    m_s[...] = jnp.full(m_s.shape, far_below, F32)
    l_s[...] = jnp.zeros(l_s.shape, F32)

    QT = min(512, SL)

    def attend(s, c0, keys, masked):
        cols = pl.ds(pl.multiple_of(c0, QT), QT)
        sc = jnp.dot(KA[s, :keys], Q2[:, cols], preferred_element_type=F32)
        if masked is not None:
            kk = lax.broadcasted_iota(jnp.int32, sc.shape, 0)
            qq = lax.broadcasted_iota(jnp.int32, sc.shape, 1) + masked
            sc = jnp.where(kk <= qq, sc, far_below)
        m_old = m_s[:, cols]
        m_new = jnp.maximum(m_old, jnp.max(sc, axis=0, keepdims=True))
        p = jnp.exp(sc - m_new)
        shrink = jnp.exp(m_old - m_new)
        m_s[:, cols] = m_new
        l_s[:, cols] = l_s[:, cols] * shrink + jnp.sum(p, axis=0, keepdims=True)
        acc[:, cols] = acc[:, cols] * shrink + jnp.dot(
            VT[s, :, :keys], p.astype(BF16), preferred_element_type=F32)

    def diag(mp, _):
        for q0 in range(0, SL, QT):
            attend(E, mp * SL + q0, q0 + QT, q0)
        return 0

    lax.fori_loop(0, 2, diag, 0)

    def kv_block(j):
        src = E - 1 - j

        @pl.when(j < E)
        def _():
            remote(KA.at[src], KA.at[src], kvsend.at[0, 0], kvrecv.at[0, src], E, T).wait_recv()
            remote(VT.at[src], VT.at[src], kvsend.at[1, 0], kvrecv.at[1, src], E, T).wait_recv()

            def tile(t, _):
                attend(src, t * QT, SL, None)
                return 0

            lax.fori_loop(0, 2 * SL // QT, tile, 0)

    def half_rows(h):
        return pl.ds(pl.multiple_of(h * HALF, HALF), HALF)

    def ag_up(zs, h, j):
        ref = X.at[zs, half_rows(h)]
        return remote(ref, ref, agus.at[j], agur.at[j], E, up_t)

    def ag_dn(zs, h, j):
        ref = X.at[zs, half_rows(h)]
        return remote(ref, ref, agds.at[j], agdr.at[j], E, dn_t)

    c_row = lax.broadcasted_iota(jnp.int32, (HALF, PS // 2), 0)
    c_col = lax.broadcasted_iota(jnp.int32, (HALF, PS // 2), 1)
    pack = jnp.zeros((HALF, PS // 2), jnp.bool_)
    for g in range(NE // 2):
        pack = pack | ((c_row >= g * CAP) & (c_row < (g + 1) * CAP) & (c_col == c_row + g * (PAD - CAP)))
    pack = pack.astype(BF16)

    for h in range(2):
        def wait_rows(s, _):
            @pl.when(s != E)
            def _():
                remote(rows_of(disp, s), rows_of(A, s), dsend.at[0], drecv.at[s], E, T).wait_recv()
            return 0

        lax.fori_loop(h * (NE // 2), (h + 1) * (NE // 2), wait_rows, 0)
        for n in range(0, DM, 512):
            nn = min(512, DM)
            X[Z, h * HALF:(h + 1) * HALF, n:n + nn] = jnp.dot(
                pack, A[h * PS // 2:(h + 1) * PS // 2, n:n + nn], preferred_element_type=F32).astype(BF16)
        if h == 0:
            ag_up(Z, 0, 0).start()
            if NZ > 2:
                ag_dn(Z, 0, 1).start()
        else:
            ag_dn(Z, 1, 0).start()
            if NZ > 2:
                ag_up(Z, 1, 1).start()

    for c in c_w:
        c.wait()
    for c in w_copies:
        c.wait_recv()

    def experts(zb):
        xb = X[zb]
        hid = []
        for w in range(2):
            g = jnp.dot(xb, wg[w], preferred_element_type=F32)
            u = jnp.dot(xb, wu[w], preferred_element_type=F32)
            hid.append((g / (1.0 + jnp.exp(-g)) * u).astype(BF16))
        for n in range(0, DM, 512):
            nn = min(512, DM)
            y = jnp.dot(hid[0], wd[0, :, n:n + nn], preferred_element_type=F32)
            y += jnp.dot(hid[1], wd[1, :, n:n + nn], preferred_element_type=F32)
            Y[zb, :, n:n + nn] = y.astype(BF16)

    def ring_parts(buf, land_u, land_d, rows, us, ur, ds_, dr):
        def place(h):
            return pl.ds(pl.multiple_of(h * rows, rows), rows)

        def up(j):
            d = (Z + NZ // 2 - (j + 1) // 2 + NZ) % NZ
            h = (j + 1) % 2
            return d, place(h), remote(buf.at[d, place(h)], land_u.at[j], us.at[j], ur.at[j], E, up_t)

        def down(j):
            d = (Z - NZ // 2 + (j + 1) // 2 + NZ) % NZ
            h = j % 2
            return d, place(h), remote(buf.at[d, place(h)], land_d.at[j], ds_.at[j], dr.at[j], E, dn_t)

        def first(j):
            up(j)[2].start()
            down(j)[2].start()

        def step(j):
            for f, land in ((up, land_u), (down, land_d)):
                f(j - 2)[2].wait_recv()
                d, where, copy = f(j)
                buf[d, where, :] = (buf[d, where, :].astype(F32) + land[j - 2].astype(F32)).astype(BF16)
                copy.start()

        def last(out):
            for j in ((NZ - 3, NZ - 2) if NZ > 2 else (0,)):
                up(j)[2].wait_recv()
                down(j)[2].wait_recv()
            for h in range(2):
                if NZ > 2:
                    ju, jd = (NZ - 3, NZ - 2) if h == 0 else (NZ - 2, NZ - 3)
                    s = buf[Z, h * rows:(h + 1) * rows, :].astype(F32) + land_u[ju].astype(F32) + land_d[jd].astype(F32)
                else:
                    s = buf[Z, h * rows:(h + 1) * rows, :].astype(F32) + (land_d[0] if h == 0 else land_u[0]).astype(F32)
                out(h, s.astype(BF16))

        def drain(j, _):
            up(j)[2].wait_send()
            down(j)[2].wait_send()
            return 0

        return first, step, last, drain

    y_first, y_step, y_last, y_drain = ring_parts(Y, RU, RD, HALF, rsus, rsur, rsds, rsdr)
    MR = ROWS // 2
    m_first, m_step, m_last, m_drain = ring_parts(MY, MRU, MRD, MR, mus, mur, mds, mdr)

    STEPS = (NZ - 1) + max(NZ - 2, 1)
    NKV = NE - 1

    def main(i, _):
        @pl.when(i < NZ - 1)
        def _():
            k = i // 2 + 1
            h = i % 2
            zu = (Z - k + NZ) % NZ
            zd = (Z + k) % NZ
            ag_up(zu, h, i).wait_recv()
            if NZ > 2:
                @pl.when(i < NZ - 3)
                def _():
                    ag_up(zu, h, i + 2).start()
            ag_dn(zd, 1 - h, i).wait_recv()
            if NZ > 2:
                @pl.when(i < NZ - 3)
                def _():
                    ag_dn(zd, 1 - h, i + 2).start()

        @pl.when(i < NZ)
        def _():
            k = (i + 1) // 2
            zb = (Z + k * (1 - 2 * (i % 2)) + NZ) % NZ
            experts(zb)

        @pl.when(i == NZ - 1)
        def _():
            y_first(0)
            if NZ > 2:
                y_first(1)

        if NZ > 2:
            @pl.when(i >= NZ)
            def _():
                y_step(i - NZ + 2)

        def blocks(j, _):
            kv_block(j)
            return 0

        lax.fori_loop((i * NKV) // STEPS, ((i + 1) * NKV) // STEPS, blocks, 0)
        return 0

    lax.fori_loop(0, STEPS, main, 0)

    o = acc[...] / l_s[...]
    comb = o[:, :SL] - lam_ref[0] * o[:, SL:]
    comb = comb * lax.rsqrt(jnp.mean(comb * comb, axis=0, keepdims=True) + epsilon)
    heads = (comb.T * gain_ref[...]).astype(BF16)
    for t in range(2 * NZ):
        hb[t % 2, (t // 2) * ROWS:(t // 2 + 1) * ROWS, :] = heads[t * ROWS:(t + 1) * ROWS, :]
    h_copy = remote(hb.at[1 - C], hx, hsend.at[0], hrecv.at[0], E, par_t)
    h_copy.start()

    u_row = lax.broadcasted_iota(jnp.int32, (PS // 2, HALF), 0)
    u_col = lax.broadcasted_iota(jnp.int32, (PS // 2, HALF), 1)
    unpack = jnp.zeros((PS // 2, HALF), jnp.bool_)
    for g in range(NE // 2):
        unpack = unpack | ((u_col >= g * CAP) & (u_col < (g + 1) * CAP) & (u_row == u_col + g * (PAD - CAP)))
    unpack = unpack.astype(BF16)

    def spread(h, s):
        for n in range(0, DM, 512):
            nn = min(512, DM)
            RET[h * PS // 2:(h + 1) * PS // 2, n:n + nn] = jnp.dot(
                unpack, s[:, n:n + nn], preferred_element_type=F32).astype(BF16)

    y_last(spread)

    def ret_copy(j):
        dst = (E + j) % NE
        return remote(rows_of(RET, dst), rows_of(B, E), rtsend.at[j], rtrecv.at[E], dst, T)

    def send_ret(j, _):
        ret_copy(j).start()
        return 0

    lax.fori_loop(1, NE, send_ret, 0)
    B[own, :] = RET[own, :]

    h_copy.wait_recv()
    for zd in range(NZ):
        ha = hb[C, zd * ROWS:(zd + 1) * ROWS, :]
        hc = hx[zd * ROWS:(zd + 1) * ROWS, :]
        for n in range(0, DM, 512):
            nn = min(512, DM)
            MY[zd, :, n:n + nn] = (jnp.dot(ha, wo[0, :, n:n + nn], preferred_element_type=F32)
                                   + jnp.dot(hc, wo[1, :, n:n + nn], preferred_element_type=F32)).astype(BF16)
    m_first(0)
    if NZ > 2:
        m_first(1)

    def wait_ret(s, _):
        @pl.when(s != E)
        def _():
            remote(rows_of(RET, s), rows_of(B, s), rtsend.at[0], rtrecv.at[s], E, T).wait_recv()
        return 0

    if NZ > 2:
        def m_loop(j, _):
            m_step(j)
            return 0

        lax.fori_loop(2, NZ - 1, m_loop, 0)

    lax.fori_loop(0, NE, wait_ret, 0)
    rw = rw_ref[...]
    for n in range(0, DM, 512):
        nn = min(512, DM)
        bb = B[:, n:n + nn]
        moe_ref[:, n:n + nn] = (
            rw[:, 0:1] * jnp.dot(sel[0], bb, preferred_element_type=F32)
            + rw[:, 1:2] * jnp.dot(sel[1], bb, preferred_element_type=F32)).astype(BF16)

    def mix_out(h, s):
        mix_ref[h * MR:(h + 1) * MR, :] = s

    m_last(mix_out)

    def drain_ep(j, _):
        disp_copy(j).wait_send()
        ret_copy(j).wait_send()

        @pl.when(E + j < NE)
        def _():
            for c in kv_copies(j):
                c.wait_send()
        return 0

    lax.fori_loop(1, NE, drain_ep, 0)
    for c in (*w_copies, h_copy):
        c.wait_send()

    def drain_z(j, _):
        ag_up(Z, 0, j).wait_send()
        ag_dn(Z, 0, j).wait_send()
        y_drain(j, 0)
        m_drain(j, 0)
        return 0

    lax.fori_loop(0, NZ - 1, drain_z, 0)


def make_body(cap):
    def body(mix_query, mix_key, mix_value, head_lambda, head_gain, out_weight, moe_input, moe_gain,
             expert_ids, route_weight, gate_weight, up_weight, down_weight):
        NE = lax.axis_size("ep")
        NZ = lax.axis_size("tp") // 2
        SL = mix_query.shape[0]
        ROWS, DM = moe_input.shape
        FFD = gate_weight.shape[2]
        CAP = cap if cap else 3 * ROWS * expert_ids.shape[1] // (2 * NE)
        pos = (lax.axis_index("ep") * SL + jnp.arange(SL, dtype=jnp.int32)).astype(F32)
        freq = rotary_base ** (-jnp.arange(32, dtype=F32) * 2.0 / 64)
        ang = freq[:, None] * pos[None, :]
        cosv, sinv = jnp.cos(ang), jnp.sin(ang)
        cfg = (NE, NZ, SL, DM, FFD, ROWS, CAP)
        SLOTS, PS = NE * CAP, NE * PAD
        HALF = SLOTS // 2
        N1 = NZ - 1
        VM, DMA = pltpu.VMEM, pltpu.SemaphoreType.DMA
        any_ = pl.BlockSpec(memory_space=pl.ANY)
        vm = pl.BlockSpec(memory_space=pltpu.VMEM)
        sm = pl.BlockSpec(memory_space=pltpu.SMEM)
        scratch = [
            VM((ROWS, DM), BF16), VM((SL, 128), BF16), VM((SL, 128), BF16), VM((SL, 128), BF16),
            VM((2, DM, FFD), BF16), VM((2, DM, FFD), BF16), VM((2, FFD, DM), BF16), VM((2, 128, DM), BF16),
            VM((PS, DM), BF16), VM((PS, DM), BF16),
            VM((NZ, SLOTS, DM), BF16), VM((NZ, SLOTS, DM), BF16),
            VM((N1, HALF, DM), BF16), VM((N1, HALF, DM), BF16),
            VM((PS, DM), BF16), VM((PS, DM), BF16),
            VM((NE, SL, 128), BF16), VM((NE, 128, SL), BF16), VM((128, 2 * SL), BF16),
            VM((128, 2 * SL), F32), VM((1, 2 * SL), F32), VM((1, 2 * SL), F32),
            VM((2, SL // 2, 128), BF16), VM((SL // 2, 128), BF16),
            VM((NZ, ROWS, DM), BF16), VM((N1, ROWS // 2, DM), BF16), VM((N1, ROWS // 2, DM), BF16),
            DMA((8,)), DMA((4,)), DMA((4,)), DMA((NE,)), DMA((NE,)), DMA((2, NE)), DMA((2, NE)),
            DMA((N1,)), DMA((N1,)), DMA((N1,)), DMA((N1,)),
            DMA((N1,)), DMA((N1,)), DMA((N1,)), DMA((N1,)),
            DMA((NE,)), DMA((NE,)), DMA((1,)), DMA((1,)),
            DMA((N1,)), DMA((N1,)), DMA((N1,)), DMA((N1,)),
        ]
        return pl.pallas_call(
            functools.partial(kernel, cfg),
            out_shape=(jax.ShapeDtypeStruct((ROWS, DM), BF16), jax.ShapeDtypeStruct((ROWS, DM), BF16)),
            in_specs=[any_, any_, any_, sm, vm, any_, any_, vm, vm, vm, any_, any_, any_, vm, vm],
            out_specs=(vm, vm),
            scratch_shapes=scratch,
            compiler_params=pltpu.CompilerParams(
                collective_id=0, has_side_effects=True, vmem_limit_bytes=67043328),
            name="step",
        )(mix_query, mix_key, mix_value, head_lambda, head_gain.reshape(1, -1), out_weight, moe_input,
          moe_gain.reshape(1, -1), expert_ids, route_weight, gate_weight, up_weight, down_weight, cosv, sinv)

    return body


def solution(mesh, cap=None):
    return jax.shard_map(
        make_body(cap),
        mesh=mesh,
        in_specs=(
            P("ep", "tp"), P("ep", "tp"), P("ep", "tp"), P("tp"), P(), P("tp", None),
            P(("ep", "tp"), None), P(), P(("ep", "tp"), None), P(("ep", "tp"), None),
            P("ep", None, "tp"), P("ep", None, "tp"), P("ep", "tp", None),
        ),
        out_specs=(P(("ep", "tp"), None), P(("ep", "tp"), None)),
        check_vma=False,
    )
```

time: 452 us -> 221 us (0.49); the launches traced: 446 us -> 221 us
  waiting for transfers between devices: 221 us -> 0 us
  Pallas kernels: 0 us -> 214 us
  matrix products: 80.7 us -> 0 us
  other arithmetic: 51.2 us -> 1.25 us
  blocking collectives: 29 us -> 0 us
  loops' own time: 22.3 us -> 0 us
  local copies, waits for them, and re-layouts: 20.2 us -> 4.5 us
  between operations: 14.6 us -> 1.32 us
  starting transfers between devices: 7.52 us -> 0 us
    pallas_call x0 -> x1, Pallas kernels: none -> 214 us  [body(): pl.pallas_call(functools.partial(kernel, cfg), out_shape=(jax.ShapeDtypeS...]
    reduce_scatter x1 -> x0, waiting for transfers between devices: 160 us -> none  [body(): lax.psum_scatter(jnp.concatenate([mixer_part, expert_part], axis=1).resha...]
    dot_general x23 -> x0, matrix products: 80.7 us -> none  [the longest x9 30.4 us: attend_block(): jnp.einsum('hpqk,khe->hpqe', expo.astype(jnp.bfloat16), value_rows, prefe...]
    all_gather x2 -> x0, waiting for transfers between devices: 48.6 us -> none  [the longest x1 48.6 us: body(): lax.all_gather(stacked, 'ep', axis=0, tiled=True)]
    all_to_all x1 -> x0, blocking collectives: 29 us -> none  [body(): lax.all_to_all(outgoing, 'ep', split_axis=2, concat_axis=0, tiled=True)]
    another operation x17 -> x0, loops' own time: 22.3 us -> none  [the longest x1 21.4 us: fold_keys(): return lax.fori_loop(0, number // step_rows, one_block, attention_state)]
    reduce_sum x13 -> x0, other arithmetic: 17.3 us -> none  [the longest x9 15.4 us: attend_block(): totals = totals * shrink + jnp.sum(expo, axis=-1)]
    concatenate x3 -> x0, other arithmetic: 15.7 us -> none  [the longest x1 13.8 us: body(): jnp.concatenate([mixer_part, expert_part], axis=1)]
  transfers between devices with their start and end apart: 4 -> 0, of which waited for: 3 -> 0; matrix products, arithmetic and copies ran while one was open for 23% -> 0% of each run, Pallas kernels for 0% -> 0%
where the time goes in v1:
time: 221 us
  Pallas kernels  214 us (97%)
  local copies, waits for them, and re-layouts  4.5 us (2%)
    pallas_call x1, Pallas kernels, body(): pl.pallas_call(functools.partial(kernel, cfg), out_shape=(jax.ShapeDtypeS...  214 us
    unnamed x10, local copies, waits for them, and re-layouts  4.5 us

profile of v1, /device:TPU:16, one launch (start us, length us, event | category | flops | bytes accessed | tf_op | source)
XLA Modules:
  0.0 221.1 jit_solution(9997764737289998281)
XLA Ops:
  1.3 0.0 copy-start.1
  1.3 0.7 copy-done.1
  2.0 0.0 copy-start.2
  2.0 0.7 copy.15.refs_8_
  2.7 0.0 copy-done.2
  2.7 0.7 copy.16.refs_9_
  3.4 1.2 multiply_sine_fusion
  4.6 214.0 %step.1 = (bf16[64,2048]{1,0:T(8,128)(2,1)}, bf16[64,2048]{1,0:T(8,128)(2,1)}) custom-call(bf16[1024,128]{1,0:T(8,128)(2,1)} %refs_0_.1, bf16[1024,128]{1,0:T(8,128)(2,1)} %refs_1_.1, bf16[1024,128]{1,0:T(8,128)(2,1)} %refs_2_.1, f32[1]{0:T(128)S(6)} %copy.19.refs_3_, f32[1,128]{1,0:T(1,128)} %bitcast.3, bf16[128,2048]{1,0:T(8,128)(2,1)} %refs_5_.1, ...), custom_call_target="tpu_custom_call" | custom-call | tf_op jit(solution)/shard_map/step/pallas_call | solution.py:488
  218.7 0.0 copy-start
  218.7 1.7 copy.20
  220.4 0.0 copy-done
  220.4 0.7 copy.21
  (2 shorter events, 0.0 us)
Async XLA Ops:
  1.3 0.7 copy-start.1
  2.0 0.7 copy-start.2
  218.7 1.7 copy-start

commit v2 on v1

--- a/solution.py
+++ b/solution.py
@@ -1,4 +1,5 @@
 import functools
+import math
 
 import jax
 import jax.numpy as jnp
@@ -11,6 +12,7 @@
 rotary_base = 10000.0
 far_below = -1e30
 MESH = pl.DeviceIdType.MESH
+scope = jax.named_scope
 F32 = jnp.float32
 BF16 = jnp.bfloat16
 PAD = 16
@@ -41,6 +43,9 @@
     up_t = 2 * ((Z + 1) % NZ) + C
     dn_t = 2 * ((Z + NZ - 1) % NZ) + C
     par_t = 2 * Z + (1 - C)
+    NX = math.isqrt(NE)
+    NY = NE // NX
+    x_at, y_at = E % NX, E // NX
     SLOTS = NE * CAP
     HALF = SLOTS // 2
     HEADS_W = 128
@@ -82,7 +87,8 @@
         slot = ids[:, j:j + 1] * PAD + rank
         sel.append((slot == slot_lane).astype(BF16))
 
-    c_x.wait()
+    with scope("xwait"):
+        c_x.wait()
     xv = xin[...].astype(F32)
     normed = (xv * lax.rsqrt(jnp.mean(xv * xv, axis=-1, keepdims=True) + epsilon) * mgain_ref[...]).astype(BF16)
     both = sel[0] + sel[1]
@@ -92,7 +98,8 @@
             both, normed[:, n:n + nn], (((0,), (0,)), ((), ())), preferred_element_type=F32
         ).astype(BF16)
 
-    pl.semaphore_wait(barrier, NE - 1 + 3)
+    with scope("barrier"):
+        pl.semaphore_wait(barrier, NE - 1 + 3)
 
     def rows_of(buf, e):
         return buf.at[pl.ds(pl.multiple_of(e * PAD, PAD), PAD)]
@@ -129,25 +136,67 @@
             parts.append(b * cosv + a * sinv)
         return jnp.concatenate(parts, axis=0)
 
-    c_k.wait()
-    kt = rotated(k_in[...].astype(F32).T)
-    KA[E] = kt.T.astype(BF16)
-    c_v.wait()
-    VT[E] = v_in[...].T
-
-    def kv_copies(j):
-        dst = (E + j) % NE
-        return (remote(KA.at[E], KA.at[E], kvsend.at[0, j], kvrecv.at[0, E], dst, T),
-                remote(VT.at[E], VT.at[E], kvsend.at[1, j], kvrecv.at[1, E], dst, T))
-
-    def send_kv(j, _):
-        @pl.when(E + j < NE)
-        def _():
-            for c in kv_copies(j):
-                c.start()
-        return 0
-
-    lax.fori_loop(1, NE, send_kv, 0)
+    with scope("kprep"):
+        c_k.wait()
+        kt = rotated(k_in[...].astype(F32).T)
+        KA[E] = kt.T.astype(BF16)
+        c_v.wait()
+        VT[E] = v_in[...].T
+
+    def pass_key(s, send, x2, y2):
+        return remote(KA.at[s], KA.at[s], kvsend.at[0, send], kvrecv.at[0, s], y2 * NX + x2, T)
+
+    def pass_value(s, send, x2, y2):
+        return remote(VT.at[s], VT.at[s], kvsend.at[1, send], kvrecv.at[1, s], y2 * NX + x2, T)
+
+    def key_down(act):
+        for y2 in range(NY):
+            @pl.when(y2 > y_at)
+            def _():
+                act(pass_key(E, NE + y2, x_at, y2))
+
+    def key_along(ys, act):
+        for x2 in range(NX):
+            @pl.when((x2 != x_at) & ((ys < y_at) | (x2 > x_at)))
+            def _():
+                act(pass_key(ys * NX + x_at, ys * NX + x2, x2, y_at))
+
+    def value_along(act):
+        for x2 in range(NX):
+            @pl.when((x2 != x_at) & ((y_at < NY - 1) | (x2 > x_at)))
+            def _():
+                act(pass_value(E, NE + x2, x2, y_at))
+
+    def value_down(xs, act):
+        for y2 in range(NY):
+            @pl.when(y2 > y_at)
+            def _():
+                act(pass_value(y_at * NX + xs, y2 * NX + xs, x_at, y2))
+
+    def start(c):
+        c.start()
+
+    def sent(c):
+        c.wait_send()
+
+    FWD = max(NX, NY) - 1
+
+    def pass_on(f):
+        ys = y_at - 1 - f
+
+        @pl.when(ys >= 0)
+        def _():
+            with scope("kfwait"):
+                pass_key(ys * NX + x_at, 0, x_at, y_at).wait_recv()
+            key_along(ys, start)
+
+        xs = (x_at + 1 + f) % NX
+
+        @pl.when((f < NX - 1) & ((y_at < NY - 1) | (xs < x_at)))
+        def _():
+            with scope("vfwait"):
+                pass_value(y_at * NX + xs, 0, x_at, y_at).wait_recv()
+            value_down(xs, start)
 
     c_q.wait()
     qt = (rotated(q_in[...].astype(F32).T) * 64 ** (-0.5)).astype(BF16)
@@ -181,21 +230,29 @@
             attend(E, mp * SL + q0, q0 + QT, q0)
         return 0
 
-    lax.fori_loop(0, 2, diag, 0)
+    with scope("diag"):
+        lax.fori_loop(0, 2, diag, 0)
 
     def kv_block(j):
         src = E - 1 - j
 
         @pl.when(j < E)
         def _():
-            remote(KA.at[src], KA.at[src], kvsend.at[0, 0], kvrecv.at[0, src], E, T).wait_recv()
-            remote(VT.at[src], VT.at[src], kvsend.at[1, 0], kvrecv.at[1, src], E, T).wait_recv()
+            with scope("kvwait"):
+                @pl.when(src % NX != x_at)
+                def _():
+                    pass_key(src, 0, x_at, y_at).wait_recv()
+
+                @pl.when(src // NX != y_at)
+                def _():
+                    pass_value(src, 0, x_at, y_at).wait_recv()
 
             def tile(t, _):
                 attend(src, t * QT, SL, None)
                 return 0
 
-            lax.fori_loop(0, 2 * SL // QT, tile, 0)
+            with scope("attend"):
+                lax.fori_loop(0, 2 * SL // QT, tile, 0)
 
     def half_rows(h):
         return pl.ds(pl.multiple_of(h * HALF, HALF), HALF)
@@ -222,7 +279,8 @@
                 remote(rows_of(disp, s), rows_of(A, s), dsend.at[0], drecv.at[s], E, T).wait_recv()
             return 0
 
-        lax.fori_loop(h * (NE // 2), (h + 1) * (NE // 2), wait_rows, 0)
+        with scope("rowswait"):
+            lax.fori_loop(h * (NE // 2), (h + 1) * (NE // 2), wait_rows, 0)
         for n in range(0, DM, 512):
             nn = min(512, DM)
             X[Z, h * HALF:(h + 1) * HALF, n:n + nn] = jnp.dot(
@@ -236,10 +294,16 @@
             if NZ > 2:
                 ag_up(Z, 1, 1).start()
 
-    for c in c_w:
-        c.wait()
-    for c in w_copies:
-        c.wait_recv()
+    key_down(start)
+    value_along(start)
+    key_along(y_at, start)
+    value_down(x_at, start)
+
+    with scope("wwait"):
+        for c in c_w:
+            c.wait()
+        for c in w_copies:
+            c.wait_recv()
 
     def experts(zb):
         xb = X[zb]
@@ -274,15 +338,18 @@
 
         def step(j):
             for f, land in ((up, land_u), (down, land_d)):
-                f(j - 2)[2].wait_recv()
+                with scope("rswait"):
+                    f(j - 2)[2].wait_recv()
                 d, where, copy = f(j)
-                buf[d, where, :] = (buf[d, where, :].astype(F32) + land[j - 2].astype(F32)).astype(BF16)
+                with scope("rsadd"):
+                    buf[d, where, :] = (buf[d, where, :].astype(F32) + land[j - 2].astype(F32)).astype(BF16)
                 copy.start()
 
         def last(out):
             for j in ((NZ - 3, NZ - 2) if NZ > 2 else (0,)):
-                up(j)[2].wait_recv()
-                down(j)[2].wait_recv()
+                with scope("lastwait"):
+                    up(j)[2].wait_recv()
+                    down(j)[2].wait_recv()
             for h in range(2):
                 if NZ > 2:
                     ju, jd = (NZ - 3, NZ - 2) if h == 0 else (NZ - 2, NZ - 3)
@@ -305,6 +372,9 @@
     STEPS = (NZ - 1) + max(NZ - 2, 1)
     NKV = NE - 1
 
+    def block_at(i):
+        return jnp.maximum(jnp.minimum(i, NZ) - FWD, 0) + 2 * jnp.maximum(i - NZ, 0)
+
     def main(i, _):
         @pl.when(i < NZ - 1)
         def _():
@@ -312,12 +382,14 @@
             h = i % 2
             zu = (Z - k + NZ) % NZ
             zd = (Z + k) % NZ
-            ag_up(zu, h, i).wait_recv()
+            with scope("agwait"):
+                ag_up(zu, h, i).wait_recv()
             if NZ > 2:
                 @pl.when(i < NZ - 3)
                 def _():
                     ag_up(zu, h, i + 2).start()
-            ag_dn(zd, 1 - h, i).wait_recv()
+            with scope("agwait2"):
+                ag_dn(zd, 1 - h, i).wait_recv()
             if NZ > 2:
                 @pl.when(i < NZ - 3)
                 def _():
@@ -327,7 +399,8 @@
         def _():
             k = (i + 1) // 2
             zb = (Z + k * (1 - 2 * (i % 2)) + NZ) % NZ
-            experts(zb)
+            with scope("experts"):
+                experts(zb)
 
         @pl.when(i == NZ - 1)
         def _():
@@ -340,15 +413,21 @@
             def _():
                 y_step(i - NZ + 2)
 
+        @pl.when(i < FWD)
+        def _():
+            pass_on(i)
+
         def blocks(j, _):
             kv_block(j)
             return 0
 
-        lax.fori_loop((i * NKV) // STEPS, ((i + 1) * NKV) // STEPS, blocks, 0)
+        lax.fori_loop(block_at(i), jnp.where(i == STEPS - 1, NKV, block_at(i + 1)), blocks, 0)
         return 0
 
     lax.fori_loop(0, STEPS, main, 0)
 
+    with scope("endloop"):
+        pass
     o = acc[...] / l_s[...]
     comb = o[:, :SL] - lam_ref[0] * o[:, SL:]
     comb = comb * lax.rsqrt(jnp.mean(comb * comb, axis=0, keepdims=True) + epsilon)
@@ -384,7 +463,8 @@
     lax.fori_loop(1, NE, send_ret, 0)
     B[own, :] = RET[own, :]
 
-    h_copy.wait_recv()
+    with scope("hwait"):
+        h_copy.wait_recv()
     for zd in range(NZ):
         ha = hb[C, zd * ROWS:(zd + 1) * ROWS, :]
         hc = hx[zd * ROWS:(zd + 1) * ROWS, :]
@@ -392,7 +472,8 @@
             nn = min(512, DM)
             MY[zd, :, n:n + nn] = (jnp.dot(ha, wo[0, :, n:n + nn], preferred_element_type=F32)
                                    + jnp.dot(hc, wo[1, :, n:n + nn], preferred_element_type=F32)).astype(BF16)
-    m_first(0)
+    with scope("mfirst"):
+        m_first(0)
     if NZ > 2:
         m_first(1)
 
@@ -409,7 +490,8 @@
 
         lax.fori_loop(2, NZ - 1, m_loop, 0)
 
-    lax.fori_loop(0, NE, wait_ret, 0)
+    with scope("retwait"):
+        lax.fori_loop(0, NE, wait_ret, 0)
     rw = rw_ref[...]
     for n in range(0, DM, 512):
         nn = min(512, DM)
@@ -426,16 +508,20 @@
     def drain_ep(j, _):
         disp_copy(j).wait_send()
         ret_copy(j).wait_send()
-
-        @pl.when(E + j < NE)
-        def _():
-            for c in kv_copies(j):
-                c.wait_send()
-        return 0
-
-    lax.fori_loop(1, NE, drain_ep, 0)
+        return 0
+
+    with scope("drain"):
+        lax.fori_loop(1, NE, drain_ep, 0)
     for c in (*w_copies, h_copy):
         c.wait_send()
+    key_down(sent)
+    value_along(sent)
+    for ys in range(NY):
+        @pl.when(ys <= y_at)
+        def _():
+            key_along(ys, sent)
+    for xs in range(NX):
+        value_down(xs, sent)
 
     def drain_z(j, _):
         ag_up(Z, 0, j).wait_send()
@@ -479,7 +565,7 @@
             VM((128, 2 * SL), F32), VM((1, 2 * SL), F32), VM((1, 2 * SL), F32),
             VM((2, SL // 2, 128), BF16), VM((SL // 2, 128), BF16),
             VM((NZ, ROWS, DM), BF16), VM((N1, ROWS // 2, DM), BF16), VM((N1, ROWS // 2, DM), BF16),
-            DMA((8,)), DMA((4,)), DMA((4,)), DMA((NE,)), DMA((NE,)), DMA((2, NE)), DMA((2, NE)),
+            DMA((8,)), DMA((4,)), DMA((4,)), DMA((NE,)), DMA((NE,)), DMA((2, 2 * NE)), DMA((2, NE)),
             DMA((N1,)), DMA((N1,)), DMA((N1,)), DMA((N1,)),
             DMA((N1,)), DMA((N1,)), DMA((N1,)), DMA((N1,)),
             DMA((NE,)), DMA((NE,)), DMA((1,)), DMA((1,)),

time: 221 us -> 193 us (0.87)
  Pallas kernels: 214 us -> 186 us
    pallas_call x1, Pallas kernels: 214 us -> 186 us  [body(): pl.pallas_call(functools.partial(kernel, cfg), out_shape=(jax.ShapeDtypeS...]
where the time goes in v2:
time: 193 us
  Pallas kernels  186 us (96%)
  local copies, waits for them, and re-layouts  4.5 us (2%)
    pallas_call x1, Pallas kernels, body(): pl.pallas_call(functools.partial(kernel, cfg), out_shape=(jax.ShapeDtypeS...  186 us
    unnamed x10, local copies, waits for them, and re-layouts  4.5 us

profile of v2, /device:TPU:16, one launch (start us, length us, event | category | flops | bytes accessed | tf_op | source)
XLA Modules:
  0.0 193.0 jit_solution(1630958262114849472)
XLA Ops:
  1.3 0.0 copy-start.1
  1.3 0.7 copy-done.1
  2.0 0.0 copy-start.2
  2.0 0.7 copy.15.refs_8_
  2.7 0.0 copy-done.2
  2.7 0.7 copy.16.refs_9_
  3.4 1.2 multiply_sine_fusion
  4.6 185.9 %step.1 = (bf16[64,2048]{1,0:T(8,128)(2,1)}, bf16[64,2048]{1,0:T(8,128)(2,1)}) custom-call(bf16[1024,128]{1,0:T(8,128)(2,1)} %refs_0_.1, bf16[1024,128]{1,0:T(8,128)(2,1)} %refs_1_.1, bf16[1024,128]{1,0:T(8,128)(2,1)} %refs_2_.1, f32[1]{0:T(128)S(6)} %copy.19.refs_3_, f32[1,128]{1,0:T(1,128)} %bitcast.3, bf16[128,2048]{1,0:T(8,128)(2,1)} %refs_5_.1, ...), custom_call_target="tpu_custom_call" | custom-call | tf_op jit(solution)/shard_map/step/pallas_call | solution.py:574
  190.6 0.0 copy-start
  190.6 1.7 copy.20
  192.3 0.0 copy-done
  192.3 0.7 copy.21
  (2 shorter events, 0.0 us)
Async XLA Ops:
  1.3 0.7 copy-start.1
  2.0 0.7 copy-start.2
  190.6 1.7 copy-start

commit v3 on v2

v3 whole, which is shorter than its diff:
```python
import functools
import math

import jax
import jax.numpy as jnp
from jax import lax
from jax.experimental import pallas as pl
from jax.experimental.pallas import tpu as pltpu
from jax.sharding import PartitionSpec as P

epsilon = 1e-06
rotary_base = 10000.0
far_below = -1e30
MESH = pl.DeviceIdType.MESH
F32 = jnp.float32
BF16 = jnp.bfloat16
scope = jax.named_scope
NQ = 4


def remote(src, dst, send, recv, ep, tp):
    return pltpu.make_async_remote_copy(
        src_ref=src, dst_ref=dst, send_sem=send, recv_sem=recv,
        device_id={"ep": ep, "tp": tp}, device_id_type=MESH,
    )


def start(c):
    c.start()


def sent(c):
    c.wait_send()


def dot(a, b):
    return jnp.dot(a, b, preferred_element_type=F32)


def iota(shape, dim):
    return lax.broadcasted_iota(jnp.int32, shape, dim)


def one(x):
    return x.astype(F32).astype(BF16)


def kernel(cfg, *refs):
    (NE, NZ, SL, DM, FFD, ROWS, CAP) = cfg
    (q_hbm, k_hbm, v_hbm, lam_ref, gain_ref, wo_hbm, x_hbm, mgain_ref, ids_ref, rw_ref,
     wg_hbm, wu_hbm, wd_hbm, freq_ref,
     mix_ref, moe_ref,
     xin, q_in, k_in, v_in, wg, wu, wd, wo, disp, A, X, Y, RU, RD, RET, B, pack, unpack,
     KA, VT, Q2, acc, m_s, l_s, S0, S1, hb, hx, MY, MRU, MRD,
     in_sem, wsend, wrecv, dsend, drecv, kvsend, kvrecv,
     agus, agur, agds, agdr, rsus, rsur, rsds, rsdr, rtsend, rtrecv, hsend, hrecv,
     mus, mur, mds, mdr) = refs

    E = lax.axis_index("ep")
    T = lax.axis_index("tp")
    Z = T // 2
    C = T % 2
    up_t = 2 * ((Z + 1) % NZ) + C
    dn_t = 2 * ((Z + NZ - 1) % NZ) + C
    par_t = 2 * Z + (1 - C)
    NX = math.isqrt(NE)
    NY = NE // NX
    x_at, y_at = E % NX, E // NX
    SLOTS = NE * CAP
    G = 4
    FC = G * CAP
    FR = NE * FC
    QC = DM // NQ
    GW = QC // G
    H2 = NZ // 2

    def local(src, dst, i):
        return pltpu.make_async_copy(src, dst, in_sem.at[i])

    c_x = local(x_hbm, xin, 0)
    c_k = local(k_hbm, k_in, 1)
    c_v = local(v_hbm, v_in, 2)
    c_q = local(q_hbm, q_in, 3)
    c_w = [local(wg_hbm.at[0], wg.at[0], 4), local(wu_hbm.at[0], wu.at[0], 5),
           local(wd_hbm.at[0], wd.at[0], 6), local(wo_hbm, wo.at[0], 7)]
    for c in (c_x, c_k, c_v, c_q, *c_w):
        c.start()

    barrier = pltpu.get_barrier_semaphore()

    def greet(j, _):
        pl.semaphore_signal(barrier, inc=1, device_id={"ep": (E + j) % NE, "tp": T}, device_id_type=MESH)
        return 0

    lax.fori_loop(1, NE, greet, 0)
    for t in (up_t, dn_t, par_t):
        pl.semaphore_signal(barrier, inc=1, device_id={"ep": E, "tp": t}, device_id_type=MESH)

    ids = ids_ref[...]
    hot = [(ids[j:j + 1, :] == iota((NE, ROWS), 0)).astype(F32) for j in range(2)]
    earlier = one(iota((ROWS, ROWS), 0) < iota((ROWS, ROWS), 1))
    before = dot((hot[0] + hot[1]).astype(BF16), earlier)
    slot = []
    for j in range(2):
        rank = jnp.sum(hot[j] * before, axis=0, keepdims=True).astype(jnp.int32)
        slot.append(ids[j:j + 1, :] * FC + rank)
    folded = [jnp.concatenate([s + g * CAP for g in range(G)], axis=1) for s in slot]
    fr = iota((FR, G * ROWS), 0)
    send_sel = one((fr == folded[0]) | (fr == folded[1]))

    with scope("xwait"):
        c_x.wait()
    xv = xin[...].astype(F32)
    normed = (xv * lax.rsqrt(jnp.mean(xv * xv, axis=-1, keepdims=True) + epsilon) * mgain_ref[...]).astype(BF16)
    for q in range(NQ):
        part = jnp.concatenate([normed[:, q * QC + g * GW:q * QC + (g + 1) * GW] for g in range(G)], axis=0)
        disp[:, q * GW:(q + 1) * GW] = dot(send_sel, part).astype(BF16)

    def fold_of(i):
        f = i.astype(F32)
        g = jnp.floor((f + 0.5) * (1.0 / SLOTS))
        t = f - g * SLOTS
        return (t + jnp.floor((t + 0.5) * (1.0 / CAP)) * (FC - CAP) + g * CAP).astype(jnp.int32)

    pack[...] = one(fold_of(iota((G * SLOTS, 1), 0)) == iota((G * SLOTS, FR), 1))
    unpack[...] = one(fold_of(iota((1, G * SLOTS), 1)) == iota((FR, G * SLOTS), 0))

    eye32 = (iota((32, 32), 0) == iota((32, 32), 1)).astype(F32)
    freq = jnp.sum(eye32 * freq_ref[...], axis=1, keepdims=True)
    pos = (iota((32, SL), 1) + E * SL).astype(F32)
    ang = freq * pos
    cosv, sinv = jnp.cos(ang), jnp.sin(ang)

    with scope("barrier"):
        pl.semaphore_wait(barrier, NE - 1 + 3)

    def rows_of(buf, e, q):
        return buf.at[pl.ds(pl.multiple_of(e * FC, FC), FC), pl.ds(q * GW, GW)]

    def others(buf, q):
        return buf.at[pl.ds(0, (NE - 1) * FC), pl.ds(q * GW, GW)]

    for q in range(NQ):
        def send_disp(j, _):
            dst = (E + j) % NE
            remote(rows_of(disp, dst, q), rows_of(A, E, q), dsend.at[q], drecv.at[q], dst, T).start()
            return 0

        lax.fori_loop(1, NE, send_disp, 0)
    own = pl.ds(pl.multiple_of(E * FC, FC), FC)
    A[own, :] = disp[own, :]

    w_copies = [
        remote(wg_hbm.at[0], wg.at[1], wsend.at[0], wrecv.at[0], E, par_t),
        remote(wu_hbm.at[0], wu.at[1], wsend.at[1], wrecv.at[1], E, par_t),
        remote(wd_hbm.at[0], wd.at[1], wsend.at[2], wrecv.at[2], E, par_t),
        remote(wo_hbm, wo.at[1], wsend.at[3], wrecv.at[3], E, par_t),
    ]
    for c in w_copies:
        c.start()

    def rotated(xt):
        parts = []
        for m in range(2):
            a = xt[64 * m:64 * m + 32, :]
            b = xt[64 * m + 32:64 * m + 64, :]
            parts.append(a * cosv - b * sinv)
            parts.append(b * cosv + a * sinv)
        return jnp.concatenate(parts, axis=0)

    with scope("kprep"):
        c_k.wait()
        kt = rotated(k_in[...].astype(F32).T)
        KA[E] = kt.T.astype(BF16)
        c_v.wait()
        VT[E] = v_in[...].T

    def pass_key(s, send, x2, y2):
        return remote(KA.at[s], KA.at[s], kvsend.at[0, send], kvrecv.at[0, s], y2 * NX + x2, T)

    def pass_value(s, send, x2, y2):
        return remote(VT.at[s], VT.at[s], kvsend.at[1, send], kvrecv.at[1, s], y2 * NX + x2, T)

    def key_down(act):
        for y2 in range(NY):
            @pl.when(y2 > y_at)
            def _():
                act(pass_key(E, NE + y2, x_at, y2))

    def key_along(ys, act):
        for x2 in range(NX):
            @pl.when((x2 != x_at) & ((ys < y_at) | (x2 > x_at)))
            def _():
                act(pass_key(ys * NX + x_at, ys * NX + x2, x2, y_at))

    def value_along(act):
        for x2 in range(NX):
            @pl.when((x2 != x_at) & ((y_at < NY - 1) | (x2 > x_at)))
            def _():
                act(pass_value(E, NE + x2, x2, y_at))

    def value_down(xs, act):
        for y2 in range(NY):
            @pl.when(y2 > y_at)
            def _():
                act(pass_value(y_at * NX + xs, y2 * NX + xs, x_at, y2))

    FWD = max(NX, NY) - 1
    P1 = NX + NY - 2

    def pass_on(f):
        ys = y_at - 1 - f

        @pl.when(ys >= 0)
        def _():
            with scope("kfwait"):
                pass_key(ys * NX + x_at, 0, x_at, y_at).wait_recv()
            key_along(ys, start)

        xs = (x_at - 1 - f + NX) % NX

        @pl.when((f < NX - 1) & ((y_at < NY - 1) | (xs < x_at)))
        def _():
            with scope("vfwait"):
                pass_value(y_at * NX + xs, 0, x_at, y_at).wait_recv()
            value_down(xs, start)

    c_q.wait()
    qt = (rotated(q_in[...].astype(F32).T) * 64 ** (-0.5)).astype(BF16)
    zero = jnp.zeros((64, SL), BF16)
    Q2[:, :SL] = jnp.concatenate([qt[:64], zero], axis=0)
    Q2[:, SL:] = jnp.concatenate([zero, qt[64:]], axis=0)
    acc[...] = jnp.zeros(acc.shape, F32)
    m_s[...] = jnp.full(m_s.shape, far_below, F32)
    l_s[...] = jnp.zeros(l_s.shape, F32)

    QT = min(512, SL)

    def diag(mp, _):
        for q0 in range(0, SL, QT):
            keys = q0 + QT
            cols = pl.ds(pl.multiple_of(mp * SL + q0, QT), QT)
            sc = dot(KA[E, :keys], Q2[:, cols])
            sc = jnp.where(iota(sc.shape, 0) <= iota(sc.shape, 1) + q0, sc, far_below)
            m_new = jnp.max(sc, axis=0, keepdims=True)
            p = jnp.exp(sc - m_new)
            m_s[:, cols] = m_new
            l_s[:, cols] = jnp.sum(p, axis=0, keepdims=True)
            acc[:, cols] = dot(VT[E, :, :keys], p.astype(BF16))
        return 0

    with scope("diag"):
        lax.fori_loop(0, 2, diag, 0)

    SB = (S0, S1)
    TILES = 2 * SL // QT

    def attend(s):
        def scores(t):
            sc = dot(KA[s], Q2[:, t * QT:(t + 1) * QT])
            SB[t % 2][...] = sc
            return jnp.max(sc, axis=0, keepdims=True)

        top = scores(0)
        for t in range(TILES):
            cols = slice(t * QT, (t + 1) * QT)
            m_old = m_s[:, cols]
            m_new = jnp.maximum(m_old, top)
            shrink = jnp.exp(m_old - m_new)
            m_s[:, cols] = m_new
            if t + 1 < TILES:
                top = scores(t + 1)
            p = jnp.exp(SB[t % 2][...] - m_new)
            l_s[:, cols] = l_s[:, cols] * shrink + jnp.sum(p, axis=0, keepdims=True)
            acc[:, cols] = acc[:, cols] * shrink + dot(VT[s], p.astype(BF16))

    def kv_block(j):
        r = j - P1
        rest = (y_at - 1 - r // max(NX - 1, 1)) * NX + (x_at + 1 + r % max(NX - 1, 1)) % NX
        near = jnp.where(j < x_at, E - 1 - j, E - (j - x_at + 1) * NX)
        src = jnp.where(r < 0, near, rest)

        @pl.when(((r < 0) & (j < x_at + y_at)) | ((r >= 0) & (r < y_at * (NX - 1))))
        def _():
            with scope("kvwait"):
                @pl.when(src % NX != x_at)
                def _():
                    pass_key(src, 0, x_at, y_at).wait_recv()

                @pl.when(src // NX != y_at)
                def _():
                    pass_value(src, 0, x_at, y_at).wait_recv()

            with scope("attend"):
                attend(src)

    def ag_up(zs, q, i):
        ref = X.at[zs, q]
        return remote(ref, ref, agus.at[i], agur.at[i], E, up_t)

    def ag_dn(zs, q, i):
        ref = X.at[zs, q]
        return remote(ref, ref, agds.at[i], agdr.at[i], E, dn_t)

    for q in range(NQ):
        with scope("rowswait"):
            remote(others(disp, q), others(A, q), dsend.at[q], drecv.at[q], E, T).wait_recv()
        rows = dot(pack[...], A[:, q * GW:(q + 1) * GW])
        for g in range(G):
            X[Z, q, :, g * GW:(g + 1) * GW] = rows[g * SLOTS:(g + 1) * SLOTS].astype(BF16)
        if NZ > 2 or q < 2:
            ag_up(Z, q, q).start()
        if NZ > 2 or q >= 2:
            ag_dn(Z, q, q if NZ > 2 else q - 2).start()

    key_down(start)
    value_along(start)
    key_along(y_at, start)
    value_down(x_at, start)

    with scope("wwait"):
        for c in c_w:
            c.wait()
        for c in w_copies:
            c.wait_recv()

    def experts(zb):
        xb = jnp.concatenate([X[zb, q] for q in range(NQ)], axis=1)
        hid = []
        for w in range(2):
            g = dot(xb, wg[w])
            u = dot(xb, wu[w])
            hid.append((g / (1.0 + jnp.exp(-g)) * u).astype(BF16))
        for q in range(NQ):
            n = slice(q * QC, (q + 1) * QC)
            Y[zb, q] = (dot(hid[0], wd[0, :, n]) + dot(hid[1], wd[1, :, n])).astype(BF16)

    def make_ring(buf, land_u, land_d, us, ur, ds_, dr):
        def target(t, sign):
            return (Z + sign * (H2 - (t + 1) // 2) + NZ) % NZ

        def up(t, i):
            far = 1 - jnp.minimum(t, 1)
            h = (t + 1) % 2 - far
            ref = buf.at[target(t, 1), 2 * h + i]
            return ref, remote(ref, land_u.at[2 * t + i], us.at[2 * t + i], ur.at[2 * t + i], E, up_t)

        def down(t, i):
            h = (t + 1) % 2
            ref = buf.at[target(t, -1), 2 * h + i]
            return ref, remote(ref, land_d.at[2 * t + i], ds_.at[2 * t + i], dr.at[2 * t + i], E, dn_t)

        def first():
            for i in range(2):
                up(0, i)[1].start()
                down(0, i)[1].start()
            if NZ > 2:
                for i in range(2):
                    up(2, i)[1].start()
                    down(1, i)[1].start()

        def step(s):
            for f, land, t in ((up, land_u, s + 1 - (2 - jnp.minimum(s, 2))), (down, land_d, s + 1)):
                for i in range(2):
                    with scope("rswait"):
                        f(s - 1, i)[1].wait_recv()
                    ref, copy = f(t, i)
                    ref[...] = (ref[...].astype(F32) + land[2 * (s - 1) + i].astype(F32)).astype(BF16)
                    copy.start()

        def last(out):
            if NZ > 2:
                for h in range(2):
                    t = NZ - 3 + h
                    for i in range(2):
                        with scope("lastwait"):
                            up(t, i)[1].wait_recv()
                            down(t, i)[1].wait_recv()
                        q = 2 * h + i
                        out(q, (buf[Z, q].astype(F32) + land_u[2 * t + i].astype(F32)
                                + land_d[2 * t + i].astype(F32)).astype(BF16))
            else:
                for q in range(NQ):
                    f, land = (up, land_u) if q < 2 else (down, land_d)
                    f(0, q % 2)[1].wait_recv()
                    out(q, (buf[Z, q].astype(F32) + land[q % 2].astype(F32)).astype(BF16))

        def drain(t, _):
            for i in range(2):
                up(t, i)[1].wait_send()
                down(t, i)[1].wait_send()
            return 0

        return first, step, last, drain

    y_first, y_step, y_last, y_drain = make_ring(Y, RU, RD, rsus, rsur, rsds, rsdr)
    m_first, m_step, m_last, m_drain = make_ring(MY, MRU, MRD, mus, mur, mds, mdr)

    AGS = NZ - 1
    FWD0 = max(min(2, AGS - FWD), 0)
    STEPS = AGS + max(NZ - 3, 0)
    NKV = NE - 1
    counts = {12: [0, 0, 1, 1, 2, 1, 1, 2, 2, 2, 2, 1]}.get(STEPS)
    if counts is None or NE != 16:
        counts = [0] * (STEPS - 1) + [NKV]

    def after(i, n):
        return jnp.clip(i - n + 1, 0, 1)

    def block_at(i):
        return sum(c * after(i, s + 1) for s, c in enumerate(counts) if c)

    def main(i, _):
        @pl.when(i < AGS)
        def _():
            k = i // 2 + 1
            h = i % 2
            zu = (Z - k + NZ) % NZ
            zd = (Z + k) % NZ
            final = after(i, AGS - 1)
            for n in range(2):
                with scope("agwait"):
                    ag_up(zu, 2 * h + n, 2 * i + n).wait_recv()
                if NZ > 2:
                    @pl.when(i < NZ - 3)
                    def _():
                        ag_up(zu, 2 * h + n, 2 * i + n + 4).start()
            hd = h + final
            for n in range(2):
                with scope("agwait2"):
                    ag_dn(zd, 2 * hd + n, 2 * i + n).wait_recv()
                if NZ > 2:
                    @pl.when((i < NZ - 4) | (i == NZ - 3))
                    def _():
                        ag_dn(zd, 2 * hd + n, 2 * i + n + 4 - 2 * after(i, NZ - 3)).start()

            @pl.when((i >= FWD0) & (i < FWD0 + FWD))
            def _():
                pass_on(i - FWD0)

            def block(b, _):
                kb = (b + 1) // 2
                with scope("experts"):
                    experts((Z + kb * (1 - 2 * (b % 2)) + NZ) % NZ)
                return 0

            lo = i + (after(i, NZ - 2) if NZ > 2 else 0)
            lax.fori_loop(lo, i + 1 + (after(i, NZ - 3) if NZ > 2 else 1), block, 0)

        @pl.when(i == AGS - 1)
        def _():
            y_first()

        if NZ > 2:
            @pl.when(i >= AGS)
            def _():
                y_step(i - AGS + 1)

        def blocks(j, _):
            kv_block(j)
            return 0

        lax.fori_loop(block_at(i), block_at(i + 1), blocks, 0)
        return 0

    lax.fori_loop(0, STEPS, main, 0)

    with scope("endloop"):
        o = acc[...] / l_s[...]
    comb = o[:, :SL] - lam_ref[0] * o[:, SL:]
    comb = comb * lax.rsqrt(jnp.mean(comb * comb, axis=0, keepdims=True) + epsilon)
    heads = (comb.T * gain_ref[...]).astype(BF16)
    for t in range(2 * NZ):
        hb[t % 2, (t // 2) * ROWS:(t // 2 + 1) * ROWS, :] = heads[t * ROWS:(t + 1) * ROWS, :]
    h_copy = remote(hb.at[1 - C], hx, hsend.at[0], hrecv.at[0], E, par_t)
    h_copy.start()

    with scope("hwait"):
        h_copy.wait_recv()
    for q in range(NQ):
        n = slice(q * QC, (q + 1) * QC)
        part = (dot(hb[C], wo[0, :, n]) + dot(hx[...], wo[1, :, n])).astype(BF16)
        for zd in range(NZ):
            MY[zd, q] = part[zd * ROWS:(zd + 1) * ROWS]
    with scope("mfirst"):
        m_first()
    def give_back(q, s):
        part = jnp.concatenate([s[:, g * GW:(g + 1) * GW] for g in range(G)], axis=0)
        RET[:, q * GW:(q + 1) * GW] = dot(unpack[...], part).astype(BF16)

        def send_ret(j, _):
            dst = (E + j) % NE
            remote(rows_of(RET, dst, q), rows_of(B, E, q), rtsend.at[q], rtrecv.at[q], dst, T).start()
            return 0

        lax.fori_loop(1, NE, send_ret, 0)

    y_last(give_back)
    B[own, :] = RET[own, :]

    if NZ > 2:
        def m_loop(s, _):
            m_step(s)
            return 0

        lax.fori_loop(1, NZ - 2, m_loop, 0)

    eye = (iota((ROWS, ROWS), 0) == iota((ROWS, ROWS), 1)).astype(F32)

    def column(row):
        return jnp.sum(eye * row, axis=1, keepdims=True)

    lane = iota((ROWS, FR), 1)
    take = []
    for j in range(2):
        sc = column(slot[j].astype(F32)).astype(jnp.int32)
        take.extend(one(lane == sc + g * CAP) for g in range(G))
    take = jnp.concatenate(take, axis=0)
    rw = rw_ref[...]
    w0, w1 = column(rw[0:1, :]), column(rw[1:2, :])
    with scope("retwait"):
        for q in range(NQ):
            remote(others(RET, q), others(B, q), rtsend.at[q], rtrecv.at[q], E, T).wait_recv()
    got = dot(take, B[...])
    for q in range(NQ):
        for g in range(G):
            a = got[g * ROWS:(g + 1) * ROWS, q * GW:(q + 1) * GW]
            b = got[(G + g) * ROWS:(G + g + 1) * ROWS, q * GW:(q + 1) * GW]
            moe_ref[:, q * QC + g * GW:q * QC + (g + 1) * GW] = (w0 * a + w1 * b).astype(BF16)

    def mix_out(q, s):
        mix_ref[:, q * QC:(q + 1) * QC] = s

    m_last(mix_out)

    with scope("drain"):
        for q in range(NQ):
            remote(others(disp, q), others(A, q), dsend.at[q], drecv.at[q], E, T).wait_send()
            remote(others(RET, q), others(B, q), rtsend.at[q], rtrecv.at[q], E, T).wait_send()
    for c in (*w_copies, h_copy):
        c.wait_send()
    key_down(sent)
    value_along(sent)
    for ys in range(NY):
        @pl.when(ys <= y_at)
        def _():
            key_along(ys, sent)
    for xs in range(NX):
        value_down(xs, sent)

    def drain_z(t, _):
        for i in range(2):
            ag_up(Z, 0, 2 * t + i).wait_send()
            ag_dn(Z, 0, 2 * t + i).wait_send()
        y_drain(t, 0)
        m_drain(t, 0)
        return 0

    lax.fori_loop(0, NZ - 1, drain_z, 0)


def make_body(cap):
    def body(mix_query, mix_key, mix_value, head_lambda, head_gain, out_weight, moe_input, moe_gain,
             expert_ids, route_weight, gate_weight, up_weight, down_weight):
        NE = lax.axis_size("ep")
        NZ = lax.axis_size("tp") // 2
        SL = mix_query.shape[0]
        ROWS, DM = moe_input.shape
        FFD = gate_weight.shape[2]
        CAP = cap if cap else 3 * ROWS * expert_ids.shape[1] // (2 * NE)
        freq = rotary_base ** (-jnp.arange(32, dtype=F32) * 2.0 / 64)
        cfg = (NE, NZ, SL, DM, FFD, ROWS, CAP)
        SLOTS, FR = NE * CAP, NE * 4 * CAP
        QC = DM // NQ
        NP = 2 * (NZ - 1)
        QT = min(512, SL)
        VM, DMA = pltpu.VMEM, pltpu.SemaphoreType.DMA
        any_ = pl.BlockSpec(memory_space=pl.ANY)
        vm = pl.BlockSpec(memory_space=pltpu.VMEM)
        sm = pl.BlockSpec(memory_space=pltpu.SMEM)
        scratch = [
            VM((ROWS, DM), BF16), VM((SL, 128), BF16), VM((SL, 128), BF16), VM((SL, 128), BF16),
            VM((2, DM, FFD), BF16), VM((2, DM, FFD), BF16), VM((2, FFD, DM), BF16), VM((2, 128, DM), BF16),
            VM((FR, QC), BF16), VM((FR, QC), BF16),
            VM((NZ, NQ, SLOTS, QC), BF16), VM((NZ, NQ, SLOTS, QC), BF16),
            VM((NP, SLOTS, QC), BF16), VM((NP, SLOTS, QC), BF16),
            VM((FR, QC), BF16), VM((FR, QC), BF16),
            VM((4 * SLOTS, FR), BF16), VM((FR, 4 * SLOTS), BF16),
            VM((NE, SL, 128), BF16), VM((NE, 128, SL), BF16), VM((128, 2 * SL), BF16),
            VM((128, 2 * SL), F32), VM((1, 2 * SL), F32), VM((1, 2 * SL), F32),
            VM((SL, QT), F32), VM((SL, QT), F32),
            VM((2, SL // 2, 128), BF16), VM((SL // 2, 128), BF16),
            VM((NZ, NQ, ROWS, QC), BF16), VM((NP, ROWS, QC), BF16), VM((NP, ROWS, QC), BF16),
            DMA((8,)), DMA((4,)), DMA((4,)), DMA((NQ,)), DMA((NQ,)), DMA((2, 2 * NE)), DMA((2, NE)),
            DMA((NP,)), DMA((NP,)), DMA((NP,)), DMA((NP,)),
            DMA((NP,)), DMA((NP,)), DMA((NP,)), DMA((NP,)),
            DMA((NQ,)), DMA((NQ,)), DMA((1,)), DMA((1,)),
            DMA((NP,)), DMA((NP,)), DMA((NP,)), DMA((NP,)),
        ]
        return pl.pallas_call(
            functools.partial(kernel, cfg),
            out_shape=(jax.ShapeDtypeStruct((ROWS, DM), BF16), jax.ShapeDtypeStruct((ROWS, DM), BF16)),
            in_specs=[any_, any_, any_, sm, vm, any_, any_, vm, vm, vm, any_, any_, any_, vm],
            out_specs=(vm, vm),
            scratch_shapes=scratch,
            compiler_params=pltpu.CompilerParams(
                collective_id=0, has_side_effects=True, vmem_limit_bytes=67043328),
            name="step",
        )(mix_query, mix_key, mix_value, head_lambda, head_gain.reshape(1, -1), out_weight, moe_input,
          moe_gain.reshape(1, -1), expert_ids.T, route_weight.T, gate_weight, up_weight, down_weight,
          freq.reshape(1, -1))

    return body


def solution(mesh, cap=None):
    return jax.shard_map(
        make_body(cap),
        mesh=mesh,
        in_specs=(
            P("ep", "tp"), P("ep", "tp"), P("ep", "tp"), P("tp"), P(), P("tp", None),
            P(("ep", "tp"), None), P(), P(("ep", "tp"), None), P(("ep", "tp"), None),
            P("ep", None, "tp"), P("ep", None, "tp"), P("ep", "tp", None),
        ),
        out_specs=(P(("ep", "tp"), None), P(("ep", "tp"), None)),
        check_vma=False,
    )
```

time: 193 us -> 166 us (0.86)
  Pallas kernels: 186 us -> 161 us
  local copies, waits for them, and re-layouts: 4.5 us -> 2.42 us
    pallas_call x1, Pallas kernels: 186 us -> 161 us  [body(): pl.pallas_call(functools.partial(kernel, cfg), out_shape=(jax.ShapeDtypeS...]
    unnamed x10 -> x4, local copies, waits for them, and re-layouts: 4.5 us -> 2.42 us
where the time goes in v3:
time: 166 us; the launch traced here: 165 us
  Pallas kernels  161 us (97%)
  local copies, waits for them, and re-layouts  2.42 us (1%)
    pallas_call x1, Pallas kernels, body(): pl.pallas_call(functools.partial(kernel, cfg), out_shape=(jax.ShapeDtypeS...  161 us

profile of v3, /device:TPU:16, one launch (start us, length us, event | category | flops | bytes accessed | tf_op | source)
XLA Modules:
  0.0 164.8 jit_solution(7916397217271400668)
XLA Ops:
  1.3 0.5 multiply_power_fusion.refs_13_
  1.8 160.5 %step.1 = (bf16[64,2048]{1,0:T(8,128)(2,1)}, bf16[64,2048]{1,0:T(8,128)(2,1)}) custom-call(bf16[1024,128]{1,0:T(8,128)(2,1)} %refs_0_.1, bf16[1024,128]{1,0:T(8,128)(2,1)} %refs_1_.1, bf16[1024,128]{1,0:T(8,128)(2,1)} %refs_2_.1, f32[1]{0:T(128)S(6)} %copy.17.refs_3_, f32[1,128]{1,0:T(1,128)} %bitcast.7, bf16[128,2048]{1,0:T(8,128)(2,1)} %refs_5_.1, ...), custom_call_target="tpu_custom_call" | custom-call | tf_op jit(solution)/shard_map/step/pallas_call | solution.py:600
  162.4 0.0 copy-start
  162.4 1.7 %copy.18 = bf16[64,2048]{1,0:T(8,128)(2,1)} copy(bf16[64,2048]{1,0:T(8,128)(2,1)} %get-tuple-element.4) | data formatting | bytes 524288
  164.1 0.0 copy-done
  164.1 0.7 copy.19
Async XLA Ops:
  162.4 1.7 %copy-start = (bf16[64,2048]{1,0:T(8,128)(2,1)S(1)}, bf16[64,2048]{1,0:T(8,128)(2,1)}, u32[]{:S(2)}) copy-start(bf16[64,2048]{1,0:T(8,128)(2,1)} %get-tuple-element.5) | copy-start | bytes 786436

commit v4 on v3

--- a/solution.py
+++ b/solution.py
@@ -16,6 +16,7 @@
 BF16 = jnp.bfloat16
 scope = jax.named_scope
 NQ = 4
+NF = 2
 
 
 def remote(src, dst, send, recv, ep, tp):
@@ -50,11 +51,11 @@
     (q_hbm, k_hbm, v_hbm, lam_ref, gain_ref, wo_hbm, x_hbm, mgain_ref, ids_ref, rw_ref,
      wg_hbm, wu_hbm, wd_hbm, freq_ref,
      mix_ref, moe_ref,
-     xin, q_in, k_in, v_in, wg, wu, wd, wo, disp, A, X, Y, RU, RD, RET, B, pack, unpack,
+     xin, q_in, k_in, v_in, wg, wu, wd, wo, disp, A, X, Y, RU, RD, RET, B, FY, FB, DY, DRU, DRD, info,
      KA, VT, Q2, acc, m_s, l_s, S0, S1, hb, hx, MY, MRU, MRD,
      in_sem, wsend, wrecv, dsend, drecv, kvsend, kvrecv,
      agus, agur, agds, agdr, rsus, rsur, rsds, rsdr, rtsend, rtrecv, hsend, hrecv,
-     mus, mur, mds, mdr) = refs
+     mus, mur, mds, mdr, isend, irecv, lsend, lrecv, dus, dur, dds, ddr) = refs
 
     E = lax.axis_index("ep")
     T = lax.axis_index("tp")
@@ -73,6 +74,9 @@
     QC = DM // NQ
     GW = QC // G
     H2 = NZ // 2
+    NL = NQ - NF
+    SG = min(4, NE)
+    GS, GF = SG * CAP, SG * FC
 
     def local(src, dst, i):
         return pltpu.make_async_copy(src, dst, in_sem.at[i])
@@ -93,8 +97,13 @@
         return 0
 
     lax.fori_loop(1, NE, greet, 0)
-    for t in (up_t, dn_t, par_t):
-        pl.semaphore_signal(barrier, inc=1, device_id={"ep": E, "tp": t}, device_id_type=MESH)
+
+    def greet_z(j, _):
+        pl.semaphore_signal(barrier, inc=1, device_id={"ep": E, "tp": (T + 2 * j) % (2 * NZ)}, device_id_type=MESH)
+        return 0
+
+    lax.fori_loop(1, NZ, greet_z, 0)
+    pl.semaphore_signal(barrier, inc=1, device_id={"ep": E, "tp": par_t}, device_id_type=MESH)
 
     ids = ids_ref[...]
     hot = [(ids[j:j + 1, :] == iota((NE, ROWS), 0)).astype(F32) for j in range(2)]
@@ -104,6 +113,7 @@
     for j in range(2):
         rank = jnp.sum(hot[j] * before, axis=0, keepdims=True).astype(jnp.int32)
         slot.append(ids[j:j + 1, :] * FC + rank)
+    info[Z] = jnp.concatenate([slot[0].astype(F32), slot[1].astype(F32), rw_ref[...]], axis=0)
     folded = [jnp.concatenate([s + g * CAP for g in range(G)], axis=1) for s in slot]
     fr = iota((FR, G * ROWS), 0)
     send_sel = one((fr == folded[0]) | (fr == folded[1]))
@@ -118,12 +128,12 @@
 
     def fold_of(i):
         f = i.astype(F32)
-        g = jnp.floor((f + 0.5) * (1.0 / SLOTS))
-        t = f - g * SLOTS
+        g = jnp.floor((f + 0.5) * (1.0 / GS))
+        t = f - g * GS
         return (t + jnp.floor((t + 0.5) * (1.0 / CAP)) * (FC - CAP) + g * CAP).astype(jnp.int32)
 
-    pack[...] = one(fold_of(iota((G * SLOTS, 1), 0)) == iota((G * SLOTS, FR), 1))
-    unpack[...] = one(fold_of(iota((1, G * SLOTS), 1)) == iota((FR, G * SLOTS), 0))
+    pack = one(fold_of(iota((GF, 1), 0)) == iota((GF, GF), 1))
+    unpack = one(fold_of(iota((1, GF), 1)) == iota((GF, GF), 0))
 
     eye32 = (iota((32, 32), 0) == iota((32, 32), 1)).astype(F32)
     freq = jnp.sum(eye32 * freq_ref[...], axis=1, keepdims=True)
@@ -132,7 +142,7 @@
     cosv, sinv = jnp.cos(ang), jnp.sin(ang)
 
     with scope("barrier"):
-        pl.semaphore_wait(barrier, NE - 1 + 3)
+        pl.semaphore_wait(barrier, NE - 1 + NZ - 1 + 1)
 
     def rows_of(buf, e, q):
         return buf.at[pl.ds(pl.multiple_of(e * FC, FC), FC), pl.ds(q * GW, GW)]
@@ -149,6 +159,15 @@
         lax.fori_loop(1, NE, send_disp, 0)
     own = pl.ds(pl.multiple_of(E * FC, FC), FC)
     A[own, :] = disp[own, :]
+
+    def info_copy(j, src):
+        return remote(info.at[src], info.at[src], isend.at[j], irecv.at[src], E, (T + 2 * j) % (2 * NZ))
+
+    def send_info(j, _):
+        info_copy(j, Z).start()
+        return 0
+
+    lax.fori_loop(1, NZ, send_info, 0)
 
     w_copies = [
         remote(wg_hbm.at[0], wg.at[1], wsend.at[0], wrecv.at[0], E, par_t),
@@ -276,7 +295,7 @@
 
     def kv_block(j):
         r = j - P1
-        rest = (y_at - 1 - r // max(NX - 1, 1)) * NX + (x_at + 1 + r % max(NX - 1, 1)) % NX
+        rest = (y_at - 1 - r // max(NX - 1, 1)) * NX + (x_at - 1 - r % max(NX - 1, 1) + NX) % NX
         near = jnp.where(j < x_at, E - 1 - j, E - (j - x_at + 1) * NX)
         src = jnp.where(r < 0, near, rest)
 
@@ -305,9 +324,10 @@
     for q in range(NQ):
         with scope("rowswait"):
             remote(others(disp, q), others(A, q), dsend.at[q], drecv.at[q], E, T).wait_recv()
-        rows = dot(pack[...], A[:, q * GW:(q + 1) * GW])
-        for g in range(G):
-            X[Z, q, :, g * GW:(g + 1) * GW] = rows[g * SLOTS:(g + 1) * SLOTS].astype(BF16)
+        for n in range(NE // SG):
+            rows = dot(pack, A[n * GF:(n + 1) * GF, q * GW:(q + 1) * GW])
+            for g in range(G):
+                X[Z, q, n * GS:(n + 1) * GS, g * GW:(g + 1) * GW] = rows[g * GS:(g + 1) * GS].astype(BF16)
         if NZ > 2 or q < 2:
             ag_up(Z, q, q).start()
         if NZ > 2 or q >= 2:
@@ -323,6 +343,11 @@
             c.wait()
         for c in w_copies:
             c.wait_recv()
+
+    def fold(parts, n):
+        rows = slice(n * GS, (n + 1) * GS)
+        return dot(unpack, jnp.concatenate(
+            [jnp.concatenate([y[rows, g * GW:(g + 1) * GW] for g in range(G)], axis=0) for y in parts], axis=1)).astype(BF16)
 
     def experts(zb):
         xb = jnp.concatenate([X[zb, q] for q in range(NQ)], axis=1)
@@ -331,72 +356,97 @@
             g = dot(xb, wg[w])
             u = dot(xb, wu[w])
             hid.append((g / (1.0 + jnp.exp(-g)) * u).astype(BF16))
+        later = []
         for q in range(NQ):
             n = slice(q * QC, (q + 1) * QC)
-            Y[zb, q] = (dot(hid[0], wd[0, :, n]) + dot(hid[1], wd[1, :, n])).astype(BF16)
-
-    def make_ring(buf, land_u, land_d, us, ur, ds_, dr):
+            y = (dot(hid[0], wd[0, :, n]) + dot(hid[1], wd[1, :, n])).astype(BF16)
+            if q < NF:
+                Y[zb, q] = y
+            else:
+                later.append(y)
+        for n in range(NE // SG):
+            FY[zb, n * GF:(n + 1) * GF, :] = fold(later, n)
+
+    def make_ring(PH, buf, land_u, land_d, us, ur, ds_, dr):
         def target(t, sign):
             return (Z + sign * (H2 - (t + 1) // 2) + NZ) % NZ
 
         def up(t, i):
             far = 1 - jnp.minimum(t, 1)
             h = (t + 1) % 2 - far
-            ref = buf.at[target(t, 1), 2 * h + i]
-            return ref, remote(ref, land_u.at[2 * t + i], us.at[2 * t + i], ur.at[2 * t + i], E, up_t)
+            ref = buf.at[target(t, 1), PH * h + i]
+            return ref, remote(ref, land_u.at[PH * t + i], us.at[PH * t + i], ur.at[PH * t + i], E, up_t)
 
         def down(t, i):
             h = (t + 1) % 2
-            ref = buf.at[target(t, -1), 2 * h + i]
-            return ref, remote(ref, land_d.at[2 * t + i], ds_.at[2 * t + i], dr.at[2 * t + i], E, dn_t)
+            ref = buf.at[target(t, -1), PH * h + i]
+            return ref, remote(ref, land_d.at[PH * t + i], ds_.at[PH * t + i], dr.at[PH * t + i], E, dn_t)
 
         def first():
-            for i in range(2):
+            for i in range(PH):
                 up(0, i)[1].start()
                 down(0, i)[1].start()
             if NZ > 2:
-                for i in range(2):
+                for i in range(PH):
                     up(2, i)[1].start()
                     down(1, i)[1].start()
 
         def step(s):
             for f, land, t in ((up, land_u, s + 1 - (2 - jnp.minimum(s, 2))), (down, land_d, s + 1)):
-                for i in range(2):
+                for i in range(PH):
                     with scope("rswait"):
                         f(s - 1, i)[1].wait_recv()
                     ref, copy = f(t, i)
-                    ref[...] = (ref[...].astype(F32) + land[2 * (s - 1) + i].astype(F32)).astype(BF16)
+                    ref[...] = (ref[...].astype(F32) + land[PH * (s - 1) + i].astype(F32)).astype(BF16)
                     copy.start()
 
         def last(out):
             if NZ > 2:
                 for h in range(2):
                     t = NZ - 3 + h
-                    for i in range(2):
+                    for i in range(PH):
                         with scope("lastwait"):
                             up(t, i)[1].wait_recv()
                             down(t, i)[1].wait_recv()
-                        q = 2 * h + i
-                        out(q, (buf[Z, q].astype(F32) + land_u[2 * t + i].astype(F32)
-                                + land_d[2 * t + i].astype(F32)).astype(BF16))
+                        q = PH * h + i
+                        out(q, (buf[Z, q].astype(F32) + land_u[PH * t + i].astype(F32)
+                                + land_d[PH * t + i].astype(F32)).astype(BF16))
             else:
-                for q in range(NQ):
-                    f, land = (up, land_u) if q < 2 else (down, land_d)
-                    f(0, q % 2)[1].wait_recv()
-                    out(q, (buf[Z, q].astype(F32) + land[q % 2].astype(F32)).astype(BF16))
+                for q in range(2 * PH):
+                    f, land = (up, land_u) if q < PH else (down, land_d)
+                    f(0, q % PH)[1].wait_recv()
+                    out(q, (buf[Z, q].astype(F32) + land[q % PH].astype(F32)).astype(BF16))
 
         def drain(t, _):
-            for i in range(2):
+            for i in range(PH):
                 up(t, i)[1].wait_send()
                 down(t, i)[1].wait_send()
             return 0
 
         return first, step, last, drain
 
-    y_first, y_step, y_last, y_drain = make_ring(Y, RU, RD, rsus, rsur, rsds, rsdr)
-    m_first, m_step, m_last, m_drain = make_ring(MY, MRU, MRD, mus, mur, mds, mdr)
+    y_first, y_step, y_last, y_drain = make_ring(NF // 2, Y, RU, RD, rsus, rsur, rsds, rsdr)
+    m_first, m_step, m_last, m_drain = make_ring(NQ // 2, MY, MRU, MRD, mus, mur, mds, mdr)
+
+    d_first, d_step, d_last, d_drain = make_ring(NL // 2, DY, DRU, DRD, dus, dur, dds, ddr)
+
+    def fold_rows(buf, zb, e):
+        return buf.at[zb, pl.ds(pl.multiple_of(e * FC, FC), FC)]
+
+    def fold_others(buf, zb):
+        return buf.at[zb, pl.ds(0, (NE - 1) * FC)]
+
+    def send_back(zb):
+        def to(j, _):
+            dst = (E + j) % NE
+            remote(fold_rows(FY, zb, dst), fold_rows(FB, zb, E), lsend.at[zb], lrecv.at[zb], dst, T).start()
+            return 0
+
+        lax.fori_loop(1, NE, to, 0)
+        FB[zb, own, :] = FY[zb, own, :]
 
     AGS = NZ - 1
+    BACK = AGS - 1
     FWD0 = max(min(2, AGS - FWD), 0)
     STEPS = AGS + max(NZ - 3, 0)
     NKV = NE - 1
@@ -445,11 +495,22 @@
                 return 0
 
             lo = i + (after(i, NZ - 2) if NZ > 2 else 0)
-            lax.fori_loop(lo, i + 1 + (after(i, NZ - 3) if NZ > 2 else 1), block, 0)
+            hi = i + 1 + (after(i, NZ - 3) if NZ > 2 else 1)
+            lax.fori_loop(lo, hi, block, 0)
 
         @pl.when(i == AGS - 1)
         def _():
             y_first()
+
+        def back(b, _):
+            kb = (b + 1) // 2
+            send_back((Z + kb * (1 - 2 * (b % 2)) + NZ) % NZ)
+            return 0
+
+        @pl.when(i == BACK)
+        def _():
+            with scope("back"):
+                lax.fori_loop(0, NZ, back, 0)
 
         if NZ > 2:
             @pl.when(i >= AGS)
@@ -475,6 +536,56 @@
     h_copy = remote(hb.at[1 - C], hx, hsend.at[0], hrecv.at[0], E, par_t)
     h_copy.start()
 
+    def give_back(q, y):
+        for n in range(NE // SG):
+            RET[n * GF:(n + 1) * GF, q * GW:(q + 1) * GW] = fold([y], n)
+
+        def send_ret(j, _):
+            dst = (E + j) % NE
+            remote(rows_of(RET, dst, q), rows_of(B, E, q), rtsend.at[q], rtrecv.at[q], dst, T).start()
+            return 0
+
+        lax.fori_loop(1, NE, send_ret, 0)
+
+    y_last(give_back)
+    B[own, :] = RET[own, :]
+
+    eye = (iota((ROWS, ROWS), 0) == iota((ROWS, ROWS), 1)).astype(F32)
+    lane = iota((ROWS, FR), 1)
+
+    def column(row):
+        return jnp.sum(eye * row, axis=1, keepdims=True)
+
+    def tokens(zb, rows, out):
+        inf = info[zb]
+        sc = [column(inf[j:j + 1, :]).astype(jnp.int32) for j in range(2)]
+        take = jnp.concatenate([one(lane == sc[j] + g * CAP) for j in range(2) for g in range(G)], axis=0)
+        w0, w1 = column(inf[2:3, :]), column(inf[3:4, :])
+        got = dot(take, rows)
+        for q in range(rows.shape[1] // GW):
+            for g in range(G):
+                a = got[g * ROWS:(g + 1) * ROWS, q * GW:(q + 1) * GW]
+                b = got[(G + g) * ROWS:(G + g + 1) * ROWS, q * GW:(q + 1) * GW]
+                out(q, g, (w0 * a + w1 * b).astype(BF16))
+
+    def dense(n, _):
+        kb = (NZ - n) // 2
+        zb = (Z + kb * (1 - 2 * (n % 2)) + NZ) % NZ
+
+        @pl.when(zb != Z)
+        def _():
+            info_copy(0, zb).wait_recv()
+
+        with scope("lwait"):
+            remote(fold_others(FY, zb), fold_others(FB, zb), lsend.at[zb], lrecv.at[zb], E, T).wait_recv()
+
+        def put(q, g, y):
+            DY[zb, q, :, g * GW:(g + 1) * GW] = y
+
+        with scope("dense"):
+            tokens(zb, FB[zb], put)
+        return 0
+
     with scope("hwait"):
         h_copy.wait_recv()
     for q in range(NQ):
@@ -484,59 +595,51 @@
             MY[zd, q] = part[zd * ROWS:(zd + 1) * ROWS]
     with scope("mfirst"):
         m_first()
-    def give_back(q, s):
-        part = jnp.concatenate([s[:, g * GW:(g + 1) * GW] for g in range(G)], axis=0)
-        RET[:, q * GW:(q + 1) * GW] = dot(unpack[...], part).astype(BF16)
-
-        def send_ret(j, _):
-            dst = (E + j) % NE
-            remote(rows_of(RET, dst, q), rows_of(B, E, q), rtsend.at[q], rtrecv.at[q], dst, T).start()
-            return 0
-
-        lax.fori_loop(1, NE, send_ret, 0)
-
-    y_last(give_back)
-    B[own, :] = RET[own, :]
-
+    lax.fori_loop(0, NZ, dense, 0)
+    d_first()
     if NZ > 2:
         def m_loop(s, _):
             m_step(s)
+            d_step(s)
             return 0
 
         lax.fori_loop(1, NZ - 2, m_loop, 0)
 
-    eye = (iota((ROWS, ROWS), 0) == iota((ROWS, ROWS), 1)).astype(F32)
-
-    def column(row):
-        return jnp.sum(eye * row, axis=1, keepdims=True)
-
-    lane = iota((ROWS, FR), 1)
-    take = []
-    for j in range(2):
-        sc = column(slot[j].astype(F32)).astype(jnp.int32)
-        take.extend(one(lane == sc + g * CAP) for g in range(G))
-    take = jnp.concatenate(take, axis=0)
-    rw = rw_ref[...]
-    w0, w1 = column(rw[0:1, :]), column(rw[1:2, :])
     with scope("retwait"):
-        for q in range(NQ):
+        for q in range(NF):
             remote(others(RET, q), others(B, q), rtsend.at[q], rtrecv.at[q], E, T).wait_recv()
-    got = dot(take, B[...])
-    for q in range(NQ):
-        for g in range(G):
-            a = got[g * ROWS:(g + 1) * ROWS, q * GW:(q + 1) * GW]
-            b = got[(G + g) * ROWS:(G + g + 1) * ROWS, q * GW:(q + 1) * GW]
-            moe_ref[:, q * QC + g * GW:q * QC + (g + 1) * GW] = (w0 * a + w1 * b).astype(BF16)
-
-    def mix_out(q, s):
-        mix_ref[:, q * QC:(q + 1) * QC] = s
+
+    def moe_part(q, g, y):
+        moe_ref[:, q * QC + g * GW:q * QC + (g + 1) * GW] = y
+
+    tokens(Z, B[...], moe_part)
+
+    def mix_out(q, y):
+        mix_ref[:, q * QC:(q + 1) * QC] = y
+
+    def moe_out(q, y):
+        moe_ref[:, (NF + q) * QC:(NF + q + 1) * QC] = y
 
     m_last(mix_out)
+    d_last(moe_out)
 
     with scope("drain"):
         for q in range(NQ):
             remote(others(disp, q), others(A, q), dsend.at[q], drecv.at[q], E, T).wait_send()
+        for q in range(NF):
             remote(others(RET, q), others(B, q), rtsend.at[q], rtrecv.at[q], E, T).wait_send()
+
+    def drain_back(zb, _):
+        remote(fold_others(FY, zb), fold_others(FB, zb), lsend.at[zb], lrecv.at[zb], E, T).wait_send()
+        return 0
+
+    lax.fori_loop(0, NZ, drain_back, 0)
+
+    def drain_info(j, _):
+        info_copy(j, Z).wait_send()
+        return 0
+
+    lax.fori_loop(1, NZ, drain_info, 0)
     for c in (*w_copies, h_copy):
         c.wait_send()
     key_down(sent)
@@ -554,6 +657,7 @@
             ag_dn(Z, 0, 2 * t + i).wait_send()
         y_drain(t, 0)
         m_drain(t, 0)
+        d_drain(t, 0)
         return 0
 
     lax.fori_loop(0, NZ - 1, drain_z, 0)
@@ -572,6 +676,7 @@
         cfg = (NE, NZ, SL, DM, FFD, ROWS, CAP)
         SLOTS, FR = NE * CAP, NE * 4 * CAP
         QC = DM // NQ
+        NL = NQ - NF
         NP = 2 * (NZ - 1)
         QT = min(512, SL)
         VM, DMA = pltpu.VMEM, pltpu.SemaphoreType.DMA
@@ -582,10 +687,12 @@
             VM((ROWS, DM), BF16), VM((SL, 128), BF16), VM((SL, 128), BF16), VM((SL, 128), BF16),
             VM((2, DM, FFD), BF16), VM((2, DM, FFD), BF16), VM((2, FFD, DM), BF16), VM((2, 128, DM), BF16),
             VM((FR, QC), BF16), VM((FR, QC), BF16),
-            VM((NZ, NQ, SLOTS, QC), BF16), VM((NZ, NQ, SLOTS, QC), BF16),
-            VM((NP, SLOTS, QC), BF16), VM((NP, SLOTS, QC), BF16),
-            VM((FR, QC), BF16), VM((FR, QC), BF16),
-            VM((4 * SLOTS, FR), BF16), VM((FR, 4 * SLOTS), BF16),
+            VM((NZ, NQ, SLOTS, QC), BF16), VM((NZ, NF, SLOTS, QC), BF16),
+            VM((NZ - 1, SLOTS, QC), BF16), VM((NZ - 1, SLOTS, QC), BF16),
+            VM((FR, NF * QC // 4), BF16), VM((FR, NF * QC // 4), BF16),
+            VM((NZ, FR, NL * QC // 4), BF16), VM((NZ, FR, NL * QC // 4), BF16),
+            VM((NZ, NL, ROWS, QC), BF16), VM((NZ - 1, ROWS, QC), BF16), VM((NZ - 1, ROWS, QC), BF16),
+            VM((NZ, 4, ROWS), F32),
             VM((NE, SL, 128), BF16), VM((NE, 128, SL), BF16), VM((128, 2 * SL), BF16),
             VM((128, 2 * SL), F32), VM((1, 2 * SL), F32), VM((1, 2 * SL), F32),
             VM((SL, QT), F32), VM((SL, QT), F32),
@@ -595,6 +702,8 @@
             DMA((NP,)), DMA((NP,)), DMA((NP,)), DMA((NP,)),
             DMA((NP,)), DMA((NP,)), DMA((NP,)), DMA((NP,)),
             DMA((NQ,)), DMA((NQ,)), DMA((1,)), DMA((1,)),
+            DMA((NP,)), DMA((NP,)), DMA((NP,)), DMA((NP,)),
+            DMA((NZ,)), DMA((NZ,)), DMA((NZ,)), DMA((NZ,)),
             DMA((NP,)), DMA((NP,)), DMA((NP,)), DMA((NP,)),
         ]
         return pl.pallas_call(

time: 166 us -> 155 us (0.934)
  Pallas kernels: 161 us -> 149 us
    pallas_call x1, Pallas kernels: 161 us -> 149 us  [body(): pl.pallas_call(functools.partial(kernel, cfg), out_shape=(jax.ShapeDtypeS...]
where the time goes in v4:
time: 155 us; the launch traced here: 154 us
  Pallas kernels  149 us (96%)
  local copies, waits for them, and re-layouts  2.42 us (2%)
    pallas_call x1, Pallas kernels, body(): pl.pallas_call(functools.partial(kernel, cfg), out_shape=(jax.ShapeDtypeS...  149 us

profile of v4, /device:TPU:16, one launch (start us, length us, event | category | flops | bytes accessed | tf_op | source)
XLA Modules:
  0.0 153.6 jit_solution(6773202139215771636)
XLA Ops:
  1.3 0.5 multiply_power_fusion.refs_13_
  1.8 149.3 %step.1 = (bf16[64,2048]{1,0:T(8,128)(2,1)}, bf16[64,2048]{1,0:T(8,128)(2,1)}) custom-call(bf16[1024,128]{1,0:T(8,128)(2,1)} %refs_0_.1, bf16[1024,128]{1,0:T(8,128)(2,1)} %refs_1_.1, bf16[1024,128]{1,0:T(8,128)(2,1)} %refs_2_.1, f32[1]{0:T(128)S(6)} %copy.17.refs_3_, f32[1,128]{1,0:T(1,128)} %bitcast.7, bf16[128,2048]{1,0:T(8,128)(2,1)} %refs_5_.1, ...), custom_call_target="tpu_custom_call" | custom-call | tf_op jit(solution)/shard_map/step/pallas_call | solution.py:709
  151.1 0.0 copy-start
  151.1 1.7 %copy.18 = bf16[64,2048]{1,0:T(8,128)(2,1)} copy(bf16[64,2048]{1,0:T(8,128)(2,1)} %get-tuple-element.4) | data formatting | bytes 524288
  152.9 0.0 copy-done
  152.9 0.7 copy.19
Async XLA Ops:
  151.1 1.7 %copy-start = (bf16[64,2048]{1,0:T(8,128)(2,1)S(1)}, bf16[64,2048]{1,0:T(8,128)(2,1)}, u32[]{:S(2)}) copy-start(bf16[64,2048]{1,0:T(8,128)(2,1)} %get-tuple-element.5) | copy-start | bytes 786436
